TPU v7x, 32 devices: a whole 2x2x4 slice. The times are simulated.
32 devices in a mesh: sp: 8 (over z, y), dp: 4 (over x, core).
Axes of the slice: x: 2, y: 2, z: 4, core: 2. Of those that a mesh axis runs over, the one named last changes fastest.
Arguments:
- tokens: bfloat16 [4, 1024, 2048], P('dp', 'sp'), may hold values from -6 to 6
- cotangent: bfloat16 [4, 1024, 2048], P('dp', 'sp'), may hold values from -6 to 6
- value_weight: bfloat16 [2048, 2048], P(('sp', 'dp')), may hold values from -0.125 to 0.125
- query_heads: bfloat16 [4, 1024, 16, 128], P('dp', None, 'sp'), may hold values from -8 to 8
- key_heads: bfloat16 [4, 1024, 16, 128], P('dp', None, 'sp'), may hold values from -8 to 8
- lambdas: float32 [16], P('sp'), may hold values from 0.3 to 0.8
Outputs:
- grad_query: bfloat16 [4, 1024, 16, 128], P('dp', None, 'sp')
- grad_key: bfloat16 [4, 1024, 16, 128], P('dp', None, 'sp')
- grad_tokens: bfloat16 [4, 1024, 2048], P('dp', 'sp')
- grad_value_weight: float32 [2048, 2048], P(('sp', 'dp'))
- grad_lambda: float32 [16], P('sp')
All inputs are finite; a program needn't handle non-finite values.
Results may differ from a plain program's by a relative error of at most 0.0095.
Values may be sent and summed in bfloat16 or wider, within the bound.
A program may use at most 192 MiB of HBM per device.

v0:
```python
import functools

import jax
import jax.numpy as jnp
from jax import lax
from jax.experimental import pallas as pl
from jax.experimental.pallas import tpu as pltpu
from jax.sharding import PartitionSpec as P

QBLOCK = 256
EPS = 1e-06
NEGATIVE = -1e30
CHUNKS = 2
F32 = jnp.float32
BF16 = jnp.bfloat16


def dot_nn(a, b):
    return jnp.dot(a, b, preferred_element_type=F32)


def dot_nt(a, b):
    return lax.dot_general(a, b, (((1,), (1,)), ((), ())), preferred_element_type=F32)


def attention_kernel(
    lam_ref, q_ref, k_ref, v_ref, g_ref, gq_ref, gk_ref, gv_ref, gl_ref, gk_acc, gv_acc
):
    length, width = q_ref.shape
    half = width // 2
    block = min(QBLOCK, length)
    scaling = half ** (-0.5)
    lam = lam_ref[pl.program_id(0)]
    lanes = lax.broadcasted_iota(jnp.int32, (length, width), 1)
    first_half = lanes < half
    q_all = q_ref[...].astype(F32) * scaling
    k_all = k_ref[...].astype(F32) * scaling
    q_halves = [
        jnp.where(first_half, q_all, 0.0).astype(BF16),
        jnp.where(first_half, 0.0, q_all).astype(BF16),
    ]
    kt_halves = [
        jnp.where(first_half, k_all, 0.0).T.astype(BF16),
        jnp.where(first_half, 0.0, k_all).T.astype(BF16),
    ]
    vt = v_ref[...].astype(F32).T.astype(BF16)
    gt = g_ref[...].astype(F32).T
    keep = lax.broadcasted_iota(jnp.int32, (block, block), 0) <= lax.broadcasted_iota(
        jnp.int32, (block, block), 1
    )
    lambda_total = jnp.zeros((1, block), F32)
    for index in range(length // block):
        off = index * block
        reach = off + block
        pieces = ([(0, off)] if off else []) + [(off, reach)]
        probs = []
        for c in range(2):
            qc = q_halves[c][off:reach]
            scores = [dot_nt(k_ref[lo:hi], qc) for lo, hi in pieces]
            scores[-1] = jnp.where(keep, scores[-1], NEGATIVE)
            top = functools.reduce(
                jnp.maximum, [jnp.max(s, axis=0, keepdims=True) for s in scores]
            )
            exps = [jnp.exp(s - top) for s in scores]
            total = sum(jnp.sum(e, axis=0, keepdims=True) for e in exps)
            inv = 1.0 / total
            probs.append([e * inv for e in exps])
        weights = [(p1 - lam * p2).astype(BF16) for p1, p2 in zip(*probs)]
        out_t = sum(dot_nn(vt[:, lo:hi], w) for (lo, hi), w in zip(pieces, weights))
        cot = gt[:, off:reach]
        inverse = lax.rsqrt(jnp.mean(out_t * out_t, axis=0, keepdims=True) + EPS)
        normed = out_t * inverse
        grad_out = (
            inverse * (cot - normed * jnp.mean(cot * normed, axis=0, keepdims=True))
        ).astype(BF16)
        grad_w = [dot_nn(v_ref[lo:hi], grad_out) for lo, hi in pieces]
        sums = [
            sum(jnp.sum(d * p, axis=0, keepdims=True) for d, p in zip(grad_w, probs[c]))
            for c in range(2)
        ]
        lambda_total = lambda_total - sums[1]
        first = [(p * (d - sums[0])).astype(BF16) for d, p in zip(grad_w, probs[0])]
        second = [(-lam * p * (d - sums[1])).astype(BF16) for d, p in zip(grad_w, probs[1])]
        gq_t = sum(
            dot_nn(kt_halves[0][:, lo:hi], a) + dot_nn(kt_halves[1][:, lo:hi], b)
            for (lo, hi), a, b in zip(pieces, first, second)
        )
        gq_ref[off:reach, :] = gq_t.T.astype(BF16)
        for (lo, hi), w, a, b in zip(pieces, weights, first, second):
            gv = dot_nt(w, grad_out)
            gk = dot_nn(a, q_halves[0][off:reach]) + dot_nn(b, q_halves[1][off:reach])
            if lo == off:
                gv_acc[lo:hi, :] = gv
                gk_acc[lo:hi, :] = gk
            else:
                gv_acc[lo:hi, :] += gv
                gk_acc[lo:hi, :] += gk
    gk_ref[...] = gk_acc[...].astype(BF16)
    gv_ref[...] = gv_acc[...].astype(BF16)
    gl_ref[...] = jnp.broadcast_to(jnp.sum(lambda_total, axis=1, keepdims=True), gl_ref.shape[1:])[
        None
    ]


def attention(lambdas, queries, keys, values, cotangent, width):
    length, features = queries.shape
    heads = features // width
    column = pl.BlockSpec((length, width), lambda h: (0, h))
    shape = jax.ShapeDtypeStruct((length, features), BF16)
    return pl.pallas_call(
        attention_kernel,
        grid=(heads,),
        in_specs=[pl.BlockSpec(memory_space=pltpu.SMEM)] + [column] * 4,
        out_specs=[column] * 3 + [pl.BlockSpec((1, 8, 128), lambda h: (h, 0, 0))],
        out_shape=[shape] * 3 + [jax.ShapeDtypeStruct((heads, 8, 128), F32)],
        scratch_shapes=[pltpu.VMEM((length, width), F32)] * 2,
        compiler_params=pltpu.CompilerParams(vmem_limit_bytes=48 * 1024 * 1024),
        cost_estimate=pl.CostEstimate(
            flops=12 * length * length * width * heads,
            bytes_accessed=14 * length * features,
            transcendentals=length * length * heads,
        ),
        name="attention",
    )(lambdas, queries, keys, values, cotangent)


def remote(src, dst, send, recv, sp, dp):
    return pltpu.make_async_remote_copy(
        src_ref=src,
        dst_ref=dst,
        send_sem=send,
        recv_sem=recv,
        device_id=(sp, dp),
        device_id_type=pl.DeviceIdType.MESH,
    )


def ring_place(sp, n):
    odd = sp % 2
    return (1 - odd) * (sp // 2) + odd * (n - 1 - sp // 2)


def ring_member(place, n):
    late = place // (n // 2)
    return (1 - late) * (2 * place) + late * (2 * (n - 1 - place) + 1)


def greet(peers):
    barrier = pltpu.get_barrier_semaphore()
    for sp, dp in peers:
        pl.semaphore_signal(
            barrier, inc=1, device_id=(sp, dp), device_id_type=pl.DeviceIdType.MESH
        )
    pl.semaphore_wait(barrier, len(peers))


def gather_kernel(
    n,
    m,
    tok_ref,
    cot_ref,
    w_ref,
    all_ref,
    coth_ref,
    wc_ref,
    local_sem,
    ring_send,
    ring_recv,
    a_send,
    a_recv,
    x_send,
    x_recv,
    c_send,
    c_recv,
):
    me = lax.axis_index("sp")
    my_dp = lax.axis_index("dp")
    rows = tok_ref.shape[0]
    feats = coth_ref.shape[2]
    part = rows // (2 * CHUNKS)
    place = ring_place(me, n)
    sides = [
        ring_member((place + 1) % n, n),
        ring_member((place + n - 1) % n, n),
    ]
    core = my_dp + 1 - 2 * (my_dp % 2)
    sp_peers = [(me + k) % n for k in range(1, n)]
    x_peers = [(my_dp + 2 * k) % m for k in range(1, m // 2)]
    greet(
        [(s, my_dp) for s in sp_peers] + [(me, d) for d in x_peers] + [(me, core)]
    )

    def columns(ref, s):
        return ref.at[:, pl.ds(pl.multiple_of(s * feats, feats), feats)]

    w_copies = [
        remote(columns(w_ref, s), wc_ref.at[me, my_dp], a_send.at[0, k], a_recv.at[0, k], s, my_dp)
        for k, s in enumerate(sp_peers)
    ]
    for copy in w_copies:
        copy.start()

    def ring(step, side, chunk):
        origin = (place + n - step) % n if side == 0 else (place + step) % n
        block = ring_member(origin, n)
        span = pl.ds((side * CHUNKS + chunk) * part, part)
        src = tok_ref.at[span] if step == 0 else all_ref.at[block, span]
        return remote(
            src,
            all_ref.at[block, span],
            ring_send.at[step, side, chunk],
            ring_recv.at[step, side, chunk],
            sides[side],
            my_dp,
        )

    order = [(side, chunk) for chunk in range(CHUNKS) for side in range(2)]
    hops = {}
    for side, chunk in order:
        hops[0, side, chunk] = ring(0, side, chunk)
        hops[0, side, chunk].start()
    locals_ = [
        pltpu.make_async_copy(tok_ref, all_ref.at[me], local_sem.at[0]),
        pltpu.make_async_copy(columns(cot_ref, me), coth_ref.at[me], local_sem.at[1]),
        pltpu.make_async_copy(columns(w_ref, me), wc_ref.at[me, my_dp], local_sem.at[2]),
    ]
    for copy in locals_:
        copy.start()
    cot_copies = [
        remote(columns(cot_ref, s), coth_ref.at[me], a_send.at[1, k], a_recv.at[1, k], s, my_dp)
        for k, s in enumerate(sp_peers)
    ]
    for copy in cot_copies:
        copy.start()
    locals_[2].wait()
    for copy in w_copies:
        copy.wait_recv()
    x_copies = [
        remote(wc_ref.at[:, my_dp], wc_ref.at[:, my_dp], x_send.at[k], x_recv.at[k], me, d)
        for k, d in enumerate(x_peers)
    ]
    for copy in x_copies:
        copy.start()
    c_copies = [remote(wc_ref.at[:, my_dp], wc_ref.at[:, my_dp], c_send.at[0], c_recv.at[0], me, core)]
    c_copies[0].start()
    for step in range(1, n - 1):
        for side, chunk in order:
            hops[step - 1, side, chunk].wait_recv()
            hops[step, side, chunk] = ring(step, side, chunk)
            hops[step, side, chunk].start()
        if step == n // 2:
            for k in range(1, m // 2):
                origin = (my_dp + m - 2 * k) % m
                x_copies[k - 1].wait_recv()
                copy = remote(
                    wc_ref.at[:, origin], wc_ref.at[:, origin], c_send.at[k], c_recv.at[k], me, core
                )
                copy.start()
                c_copies.append(copy)
    for side, chunk in order:
        hops[n - 2, side, chunk].wait_recv()
    for copy in cot_copies + c_copies:
        copy.wait_recv()
    for copy in list(hops.values()) + w_copies + cot_copies + x_copies + c_copies:
        copy.wait_send()
    locals_[0].wait()
    locals_[1].wait()


def gather(tokens, cotangent, weight, n, m):
    rows, depth = tokens.shape
    feats = weight.shape[1] // n
    vmem = pl.BlockSpec(memory_space=pltpu.VMEM)
    dma = pltpu.SemaphoreType.DMA
    return pl.pallas_call(
        functools.partial(gather_kernel, n, m),
        out_shape=[
            jax.ShapeDtypeStruct((n, rows, depth), BF16),
            jax.ShapeDtypeStruct((n, rows, feats), BF16),
            jax.ShapeDtypeStruct((n, m, weight.shape[0], feats), BF16),
        ],
        in_specs=[vmem] * 3,
        out_specs=[vmem] * 3,
        scratch_shapes=[
            dma((3,)),
            dma((n - 1, 2, CHUNKS)),
            dma((n - 1, 2, CHUNKS)),
            dma((2, n - 1)),
            dma((2, n - 1)),
            dma((max(m // 2 - 1, 1),)),
            dma((max(m // 2 - 1, 1),)),
            dma((m // 2,)),
            dma((m // 2,)),
        ],
        compiler_params=pltpu.CompilerParams(
            collective_id=0, has_side_effects=True, vmem_limit_bytes=40 * 1024 * 1024
        ),
        cost_estimate=pl.CostEstimate(
            flops=40_000_000_000, bytes_accessed=20_000_000, transcendentals=0
        ),
        name="gather",
    )(tokens, cotangent, weight)


def scatter_kernel(
    n, m, part_ref, t_ref, gl_ref, gt_ref, gw_ref, glo_ref, rbuf, sbuf, fbuf, lbuf, rs_recv, rs_send,
    local_sem, ring_send, ring_recv, t_send, t_recv, l_send, l_recv, f_send, f_recv,
):
    me = lax.axis_index("sp")
    my_dp = lax.axis_index("dp")
    rows = gt_ref.shape[0]
    feats = t_ref.shape[3]
    part = rows // (2 * CHUNKS)
    place = ring_place(me, n)
    sides = [
        ring_member((place + 1) % n, n),
        ring_member((place + n - 1) % n, n),
    ]
    sp_peers = [(me + k) % n for k in range(1, n)]
    dp_peers = [(my_dp + k) % m for k in range(1, m)]
    greet([(s, my_dp) for s in sp_peers] + [(me, d) for d in dp_peers])

    def span(side, chunk):
        return pl.ds((side * CHUNKS + chunk) * part, part)

    def own_rows(step, side, chunk):
        goal = (place + 2 * n - 1 - step) % n if side == 0 else (place + 1 + step) % n
        start = ring_member(goal, n) * rows + (side * CHUNKS + chunk) * part
        return pl.ds(pl.multiple_of(start, part), part)

    def ring(step, side, chunk):
        if step == 0:
            src = part_ref.at[own_rows(0, side, chunk)]
        else:
            src = rs_send.at[step - 1, span(side, chunk)]
        return remote(
            src,
            rs_recv.at[step, span(side, chunk)],
            ring_send.at[step, side, chunk],
            ring_recv.at[step, side, chunk],
            sides[side],
            my_dp,
        )

    order = [(side, chunk) for chunk in range(CHUNKS) for side in range(2)]
    hops = {}
    for side, chunk in order:
        hops[0, side, chunk] = ring(0, side, chunk)
        hops[0, side, chunk].start()
    t_copies = [
        remote(t_ref.at[d], rbuf.at[k], t_send.at[k], t_recv.at[k], me, d)
        for k, d in enumerate(dp_peers)
    ]
    l_copies = [
        remote(gl_ref, lbuf.at[k], l_send.at[k], l_recv.at[k], me, d)
        for k, d in enumerate(dp_peers)
    ]
    for copy in l_copies + t_copies:
        copy.start()
    f_copies = [
        remote(sbuf.at[s], fbuf.at[me], f_send.at[k], f_recv.at[k], s, my_dp)
        for k, s in enumerate(sp_peers)
    ]
    own_f = pltpu.make_async_copy(sbuf.at[me], fbuf.at[me], local_sem.at[0])
    for step in range(1, n):
        for side, chunk in order:
            hops[step - 1, side, chunk].wait_recv()
            total = rs_recv[step - 1, span(side, chunk)].astype(F32)
            total = total + part_ref[own_rows(step, side, chunk)].astype(F32)
            if step < n - 1:
                rs_send[step - 1, span(side, chunk)] = total.astype(BF16)
                hops[step, side, chunk] = ring(step, side, chunk)
                hops[step, side, chunk].start()
            else:
                gt_ref[span(side, chunk)] = total.astype(BF16)
        if step == n // 2 - 1:
            for copy in t_copies:
                copy.wait_recv()
            term = t_ref[my_dp].astype(F32)
            for k in range(m - 1):
                term = term + rbuf[k].astype(F32)
            sbuf[...] = term.astype(BF16)
            for copy in f_copies:
                copy.start()
            own_f.start()
    for copy in l_copies:
        copy.wait_recv()
    lam = gl_ref[...]
    for k in range(m - 1):
        lam = lam + lbuf[k]
    glo_ref[...] = lam
    own_f.wait()
    for copy in f_copies:
        copy.wait_recv()
    for s in range(n):
        gw_ref[:, s * feats : (s + 1) * feats] = fbuf[s].astype(F32)
    for copy in list(hops.values()) + l_copies + t_copies + f_copies:
        copy.wait_send()


def scatter(partial, term, grad_lambda, n, m):
    length, depth = partial.shape
    row_count, feats = term.shape[2:]
    rows = length // n
    vmem = pl.BlockSpec(memory_space=pltpu.VMEM)
    dma = pltpu.SemaphoreType.DMA
    return pl.pallas_call(
        functools.partial(scatter_kernel, n, m),
        out_shape=[
            jax.ShapeDtypeStruct((rows, depth), BF16),
            jax.ShapeDtypeStruct((row_count, n * feats), F32),
            jax.ShapeDtypeStruct(grad_lambda.shape, F32),
        ],
        in_specs=[vmem] * 3,
        out_specs=[vmem] * 3,
        scratch_shapes=[
            pltpu.VMEM((m - 1,) + term.shape[1:], BF16),
            pltpu.VMEM(term.shape[1:], BF16),
            pltpu.VMEM(term.shape[1:], BF16),
            pltpu.VMEM((m - 1,) + grad_lambda.shape, F32),
            pltpu.VMEM((n - 1, rows, depth), BF16),
            pltpu.VMEM((max(n - 2, 1), rows, depth), BF16),
            dma((1,)),
            dma((n - 1, 2, CHUNKS)),
            dma((n - 1, 2, CHUNKS)),
            dma((m - 1,)),
            dma((m - 1,)),
            dma((m - 1,)),
            dma((m - 1,)),
            dma((n - 1,)),
            dma((n - 1,)),
        ],
        compiler_params=pltpu.CompilerParams(
            collective_id=1, has_side_effects=True, vmem_limit_bytes=48 * 1024 * 1024
        ),
        name="scatter",
    )(partial, term, grad_lambda)


def body(n, m, tokens, cotangent, value_weight, query_heads, key_heads, lambdas):
    row_count, feature_count = value_weight.shape
    all_tokens, cotan_heads, weight_cols = gather(tokens[0], cotangent[0], value_weight, n, m)
    feats = feature_count // n
    depth = n * m * row_count
    length = all_tokens.shape[0] * all_tokens.shape[1]
    head_count, width = query_heads.shape[2], query_heads.shape[3]
    flat_tokens = all_tokens.reshape(length, depth)
    weight_cols = weight_cols.reshape(depth, feats)
    values = jnp.dot(flat_tokens, weight_cols, preferred_element_type=F32).astype(BF16)
    grad_query, grad_key, grad_value, grad_lambda = attention(
        lambdas,
        query_heads.reshape(length, feats),
        key_heads.reshape(length, feats),
        values,
        cotan_heads.reshape(length, feats),
        width,
    )
    term = lax.dot_general(
        flat_tokens, grad_value, (((0,), (0,)), ((), ())), preferred_element_type=F32
    ).astype(BF16)
    term = term.reshape(n, m, row_count, feats).transpose(1, 0, 2, 3)
    partial = dot_nt(grad_value, weight_cols).astype(BF16)
    grad_tokens, grad_weight, lambda_sum = scatter(partial, term, grad_lambda, n, m)
    return (
        grad_query.reshape(1, length, head_count, width),
        grad_key.reshape(1, length, head_count, width),
        grad_tokens[None],
        grad_weight,
        lambda_sum[:, 0, 0],
    )


def solution(mesh):
    placed = (
        P("dp", "sp", None),
        P("dp", "sp", None),
        P(("sp", "dp"), None),
        P("dp", None, "sp", None),
        P("dp", None, "sp", None),
        P("sp"),
    )
    return jax.shard_map(
        functools.partial(body, mesh.shape["sp"], mesh.shape["dp"]),
        mesh=mesh,
        in_specs=placed,
        out_specs=(
            P("dp", None, "sp", None),
            P("dp", None, "sp", None),
            P("dp", "sp", None),
            P(("sp", "dp"), None),
            P("sp"),
        ),
        check_vma=False,
    )
```

profile of v0, /device:TPU:0, one launch (start us, length us, event | category | flops | bytes accessed | tf_op | source)
XLA Modules:
  0.0 143.6 jit_solution(13147543404560112047)
XLA Ops:
  0.6 1.4 copy_bitcast_fusion.1
  2.0 0.0 copy-start.1
  2.0 1.0 copy-done.1
  3.0 0.0 copy-start.2
  3.0 1.0 copy-done.2
  4.1 0.0 copy-start.3
  4.1 0.9 copy-done.3
  5.0 63.3 %gather.1 = (bf16[8,128,2048]{2,1,0:T(8,128)(2,1)S(1)}, bf16[8,128,256]{2,1,0:T(8,128)(2,1)S(1)}, bf16[8,4,64,256]{3,2,1,0:T(8,128)(2,1)S(1)}) custom-call(bf16[128,2048]{1,0:T(8,128)(2,1)S(1)} %bitcast.28, bf16[128,2048]{1,0:T(8,128)(2,1)S(1)} %bitcast.29, bf16[64,2048]{1,0:T(8,128)(2,1)S(1)} %copy-done.3), custom_call_target="tpu_custom_call" | custom-call | flops 40000000000 | bytes 20000000 | tf_op jit(solution)/shard_map/gather/pallas_call | solution.py:275
  68.3 0.0 copy-start.4
  68.4 1.2 convolution_convert_fusion.2.v_ref
  69.6 0.0 copy-done.4
  69.6 13.0 %attention.1 = (bf16[1024,256]{1,0:T(8,128)(2,1)S(1)}, bf16[1024,256]{1,0:T(8,128)(2,1)S(1)}, bf16[1024,256]{1,0:T(8,128)(2,1)S(1)}, f32[2,8,128]{2,1,0:T(8,128)S(1)}) custom-call(f32[2]{0:T(128)S(1)} %copy-done.4, bf16[1024,256]{1,0:T(8,128)(2,1)S(1)} %get-tuple-element.26.q_ref, bf16[1024,256]{1,0:T(8,128)(2,1)S(1)} %get-tuple-element.25.k_ref, ...), custom_call_target="tpu_custom_call" | custom-call | flops 3221225472 | bytes 3670016 | tf_op jit(solution)/shard_map/attention/pallas_call | solution.py:110
  82.6 0.0 copy-start
  82.6 1.3 convolution_convert_fusion.1
  83.9 0.0 copy-done
  84.0 0.1 copy.17
  84.0 2.0 %reshape.39 = bf16[1,1024,2,128]{3,2,1,0:T(2,128)(2,1)} reshape(bf16[1024,256]{1,0:T(8,128)(2,1)} %copy-done) | data formatting | bytes 1048576 | tf_op jit(solution)/shard_map/reshape | solution.py:465
  86.0 0.9 reshape.40
  86.9 3.2 %convolution_convert_fusion.part_ref = bf16[1024,2048]{1,0:T(8,128)(2,1)} fusion(bf16[1024,256]{1,0:T(8,128)(2,1)S(1)} %get-tuple-element.20, bf16[2048,256]{1,0:T(8,128)(2,1)S(1)} %bitcast.26), kind=kOutput, calls=%fused_computation | convolution fusion | flops 1075838976 | bytes 5767168 | tf_op jit(solution)/shard_map/dot_general | solution.py:23
  90.1 51.3 %scatter.1 = (bf16[128,2048]{1,0:T(8,128)(2,1)S(1)}, f32[64,2048]{1,0:T(8,128)S(1)}, f32[2,8,128]{2,1,0:T(8,128)S(1)}) custom-call(bf16[1024,2048]{1,0:T(8,128)(2,1)} %convolution_convert_fusion.part_ref, bf16[4,8,64,256]{3,2,1,0:T(8,128)(2,1)S(1)} %bitcast.24, f32[2,8,128]{2,1,0:T(8,128)S(1)} %get-tuple-element.21.gl_ref), custom_call_target="tpu_custom_call" | custom-call | tf_op jit(solution)/shard_map/scatter/pallas_call | solution.py:407
  141.4 0.6 slice_reduce_fusion
  142.0 0.8 copy.20
  142.8 0.8 copy.21
Async XLA Ops:
  2.0 1.0 copy-start.1
  3.0 1.0 copy-start.2
  4.1 0.9 copy-start.3
  68.3 1.3 copy-start.4
  82.6 1.4 copy-start
where the time goes:
time: 144 us
  Pallas kernels  128 us (89%)
  local copies, waits for them, and re-layouts  9.54 us (7%)
  matrix products  5.81 us (4%)
    pallas_call x1, Pallas kernels, gather(): pl.pallas_call(functools.partial(gather_kernel, n, m), out_shape=[jax.Sha...  63.3 us
    pallas_call x1, Pallas kernels, scatter(): pl.pallas_call(functools.partial(scatter_kernel, n, m), out_shape=[jax.Sh...  51.3 us
    pallas_call x1, Pallas kernels, attention(): pl.pallas_call(attention_kernel, grid=(heads,), in_specs=[pl.BlockSpec(me...  13 us
    unnamed x12, local copies, waits for them, and re-layouts  4.63 us
    dot_general x1, matrix products, dot_nt(): lax.dot_general(a, b, (((1,), (1,)), ((), ())), preferred_element_type=F32)  3.23 us

commit v1 on v0

v1 whole, which is shorter than its diff:
```python
import functools

import jax
import jax.numpy as jnp
from jax import lax
from jax.experimental import pallas as pl
from jax.experimental.pallas import tpu as pltpu
from jax.sharding import PartitionSpec as P

QBLOCK = 256
EPS = 1e-06
NEGATIVE = -1e30
CHUNKS = 4
F32 = jnp.float32
BF16 = jnp.bfloat16


def dot_nn(a, b):
    return jnp.dot(a, b, preferred_element_type=F32)


def dot_nt(a, b):
    return lax.dot_general(a, b, (((1,), (1,)), ((), ())), preferred_element_type=F32)


def remote(src, dst, send, recv, sp, dp):
    return pltpu.make_async_remote_copy(
        src_ref=src,
        dst_ref=dst,
        send_sem=send,
        recv_sem=recv,
        device_id=(sp, dp),
        device_id_type=pl.DeviceIdType.MESH,
    )


def greet(peers):
    barrier = pltpu.get_barrier_semaphore()
    for sp, dp in peers:
        pl.semaphore_signal(
            barrier, inc=1, device_id=(sp, dp), device_id_type=pl.DeviceIdType.MESH
        )
    pl.semaphore_wait(barrier, len(peers))


class Attention:
    def __init__(self, lam_ref, q_ref, k_ref, v_ref, g_ref, bufs, outs, width):
        self.lam_ref, self.q_ref, self.k_ref = lam_ref, q_ref, k_ref
        self.v_ref, self.g_ref, self.width = v_ref, g_ref, width
        self.p_ref, self.a_ref, self.qh_ref, self.kt_ref, self.go_ref = bufs[:5]
        self.gv_acc, self.gk_acc = bufs[5:]
        self.gq_ref, self.gk_ref, self.gl_ref = outs
        self.length = q_ref.shape[0]
        self.block = min(QBLOCK, self.length)
        self.count = self.length // self.block

    def span(self, index):
        off = index * self.block
        reach = off + self.block
        pieces = ([(0, off)] if off else []) + [(off, reach)]
        base = self.block * (index * (index + 1) // 2)
        return off, reach, pieces, base

    def columns(self, head):
        return slice(head * self.width, (head + 1) * self.width)

    def prepare(self, head):
        length, width = self.length, self.width
        half = width // 2
        scaling = half ** (-0.5)
        lanes = lax.broadcasted_iota(jnp.int32, (length, width), 1)
        first_half = lanes < half
        q_all = self.q_ref[:, self.columns(head)].astype(F32) * scaling
        k_all = self.k_ref[:, self.columns(head)].astype(F32) * scaling
        self.qh_ref[head, 0] = jnp.where(first_half, q_all, 0.0).astype(BF16)
        self.qh_ref[head, 1] = jnp.where(first_half, 0.0, q_all).astype(BF16)
        self.kt_ref[head, 0] = jnp.where(first_half, k_all, 0.0).T.astype(BF16)
        self.kt_ref[head, 1] = jnp.where(first_half, 0.0, k_all).T.astype(BF16)

    def softmaxes(self, head, index):
        block = self.block
        lam = self.lam_ref[head]
        keep = lax.broadcasted_iota(jnp.int32, (block, block), 0) <= lax.broadcasted_iota(
            jnp.int32, (block, block), 1
        )
        off, reach, pieces, base = self.span(index)
        probs = []
        for c in range(2):
            qc = self.qh_ref[head, c, off:reach]
            scores = [dot_nt(self.k_ref[lo:hi, self.columns(head)], qc) for lo, hi in pieces]
            scores[-1] = jnp.where(keep, scores[-1], NEGATIVE)
            top = functools.reduce(
                jnp.maximum, [jnp.max(s, axis=0, keepdims=True) for s in scores]
            )
            exps = [jnp.exp(s - top) for s in scores]
            total = sum(jnp.sum(e, axis=0, keepdims=True) for e in exps)
            inv = 1.0 / total
            probs.append([e * inv for e in exps])
            for (lo, hi), p in zip(pieces, probs[c]):
                self.p_ref[head, c, base + lo : base + hi] = p
        for (lo, hi), p1, p2 in zip(pieces, *probs):
            self.a_ref[head, base + lo : base + hi] = (p1 - lam * p2).astype(BF16)

    def values_grad(self, head):
        width = self.width
        v_all = self.v_ref[:, :, :, self.columns(head)].reshape(self.length, width)
        vt = v_all.astype(F32).T.astype(BF16)
        gt = self.g_ref[:, :, self.columns(head)].reshape(self.length, width).astype(F32).T
        for index in range(self.count):
            off, reach, pieces, base = self.span(index)
            weights = self.a_ref[head, base : base + reach]
            out_t = dot_nn(vt[:, :reach], weights)
            cot = gt[:, off:reach]
            inverse = lax.rsqrt(jnp.mean(out_t * out_t, axis=0, keepdims=True) + EPS)
            normed = out_t * inverse
            grad_out = (
                inverse * (cot - normed * jnp.mean(cot * normed, axis=0, keepdims=True))
            ).astype(BF16)
            self.go_ref[head, :, off:reach] = grad_out
            gv = dot_nt(weights, grad_out)
            if off:
                self.gv_acc[0:off] += gv[0:off]
            self.gv_acc[off:reach] = gv[off:reach]

    def scores_grad(self, head):
        block, width = self.block, self.width
        lam = self.lam_ref[head]
        v_all = self.v_ref[:, :, :, self.columns(head)].reshape(self.length, width)
        lambda_total = jnp.zeros((1, block), F32)
        for index in range(self.count):
            off, reach, pieces, base = self.span(index)
            grad_out = self.go_ref[head, :, off:reach]
            probs = [
                [self.p_ref[head, c, base + lo : base + hi] for lo, hi in pieces]
                for c in range(2)
            ]
            grad_w = [dot_nn(v_all[lo:hi], grad_out) for lo, hi in pieces]
            sums = [
                sum(jnp.sum(d * p, axis=0, keepdims=True) for d, p in zip(grad_w, probs[c]))
                for c in range(2)
            ]
            lambda_total = lambda_total - sums[1]
            first = [(p * (d - sums[0])).astype(BF16) for d, p in zip(grad_w, probs[0])]
            second = [(-lam * p * (d - sums[1])).astype(BF16) for d, p in zip(grad_w, probs[1])]
            gq_t = sum(
                dot_nn(self.kt_ref[head, 0, :, lo:hi], a)
                + dot_nn(self.kt_ref[head, 1, :, lo:hi], b)
                for (lo, hi), a, b in zip(pieces, first, second)
            )
            self.gq_ref[off:reach, self.columns(head)] = gq_t.T.astype(BF16)
            for (lo, hi), a, b in zip(pieces, first, second):
                gk = dot_nn(a, self.qh_ref[head, 0, off:reach]) + dot_nn(
                    b, self.qh_ref[head, 1, off:reach]
                )
                if lo == off:
                    self.gk_acc[lo:hi, :] = gk
                else:
                    self.gk_acc[lo:hi, :] += gk
        self.gk_ref[:, self.columns(head)] = self.gk_acc[...].astype(BF16)
        self.gl_ref[head] = jnp.broadcast_to(
            jnp.sum(lambda_total, axis=1, keepdims=True), self.gl_ref.shape[1:]
        )


def whole_kernel(
    n, m, width,
    lam_ref, tok_ref, cot_ref, w_ref, q_ref, k_ref,
    gq_ref, gk_ref, gt_ref, gw_ref, glo_ref,
    tokens, tok_t, wc, coth, vloc, v_ref, p_ref, a_ref, qh_ref, kt_ref, go_ref, gv_acc, gk_acc,
    gvb, dv, part, ry, sz, rz, term, ra, sa, rb, sb, rc, sc, rd, gl_ref, lbuf,
    local_sem, wa_s, wa_r, wb_s, wb_r, wx_s, wx_r, wd_s, wd_r, tz_s, tz_r, ty_s, ty_r,
    c_s, c_r, v_s, v_r, dv_s, dv_r, y_s, y_r, z_s, z_r, a_s, a_r, b_s, b_r, e_s, e_r,
    d_s, d_r, l_s, l_r,
):
    me = lax.axis_index("sp")
    dp = lax.axis_index("dp")
    place = n // 2
    levels = place // 2
    spans = m // 2
    half, pos = me // place, me % place
    level, y = pos // 2, pos % 2
    x, core = dp // 2, dp % 2
    heads = lam_ref.shape[0]
    rows, depth = tok_ref.shape
    feats = q_ref.shape[1]
    part_rows = rows // CHUNKS
    partner = (1 - half) * place + pos
    beside = me + 1 - 2 * y
    other = dp + 1 - 2 * core

    def at_pos(p):
        return half * place + p

    ups = [(level + k) % levels for k in range(1, levels)]
    xs = [(x + k) % spans for k in range(1, spans)]
    in_half = [(pos + k) % place for k in range(1, place)]
    sp_peers = [(me + k) % n for k in range(1, n)]
    dp_peers = [(dp + k) % m for k in range(1, m)]
    done = []

    def lane(start, size):
        return pl.ds(pl.multiple_of(start, size), size)

    locals_ = [
        pltpu.make_async_copy(tok_ref, tokens.at[pos], local_sem.at[0]),
        pltpu.make_async_copy(cot_ref.at[:, lane(me * feats, feats)], coth.at[me], local_sem.at[1]),
    ] + [
        pltpu.make_async_copy(
            w_ref.at[:, lane((j * place + pos) * feats, feats)],
            wc.at[me, dp, :, pl.ds(j * feats, feats)],
            local_sem.at[2 + j],
        )
        for j in range(2)
    ]
    for copy in locals_:
        copy.start()
    greet([(s, dp) for s in sp_peers] + [(me, d) for d in dp_peers])

    def begin(copy):
        copy.start()
        done.append(copy)
        return copy

    wa = [
        begin(
            remote(
                w_ref.at[:, lane((j * place + p) * feats, feats)],
                wc.at[me, dp, :, pl.ds(j * feats, feats)],
                wa_s.at[k, j],
                wa_r.at[k, j],
                at_pos(p),
                dp,
            )
        )
        for k, p in enumerate(in_half)
        for j in range(2)
    ]

    def chunk(c):
        return pl.ds(c * part_rows, part_rows)

    def tok_up(k, c):
        return begin(
            remote(
                tok_ref.at[chunk(c)],
                tokens.at[pos, chunk(c)],
                tz_s.at[k, c],
                tz_r.at[k, c],
                at_pos(ups[k] * 2 + y),
                dp,
            )
        )

    def tok_own(c):
        return begin(
            remote(
                tok_ref.at[chunk(c)],
                tokens.at[pos, chunk(c)],
                ty_s.at[0, c],
                ty_r.at[0, c],
                beside,
                dp,
            )
        )

    def tok_side(k, c):
        origin = ((level + levels - k - 1) % levels) * 2 + y
        return begin(
            remote(
                tokens.at[origin, chunk(c)],
                tokens.at[origin, chunk(c)],
                ty_s.at[k + 1, c],
                ty_r.at[k + 1, c],
                beside,
                dp,
            )
        )

    up, own, side = {}, {}, {}
    early = CHUNKS // 2
    for c in range(early):
        for k in range(levels - 1):
            up[k, c] = tok_up(k, c)
        own[c] = tok_own(c)

    att = Attention(
        lam_ref, q_ref, k_ref, v_ref, coth,
        (p_ref, a_ref, qh_ref, kt_ref, go_ref, gv_acc, gk_acc),
        (gq_ref, gk_ref, gl_ref), width,
    )
    pieces = [(h, i) for h in range(heads) for i in range(att.count)]
    for h in range(heads):
        att.prepare(h)
    first = len(pieces) // 2
    for h, i in pieces[:first]:
        att.softmaxes(h, i)

    def wc_block(h, d):
        return wc.at[pl.ds(h * place, place), d]

    for copy in locals_[2:]:
        copy.wait()
    for copy in wa:
        copy.wait_recv()
    mine = wc_block(half, dp)
    wb = [begin(remote(mine, mine, wb_s.at[0], wb_r.at[0], partner, dp))]
    wx = [
        begin(remote(mine, mine, wx_s.at[0, k], wx_r.at[0, k], me, xk * 2 + core))
        for k, xk in enumerate(xs)
    ]
    wd = [begin(remote(mine, mine, wd_s.at[0], wd_r.at[0], me, other))]
    for c in range(early, CHUNKS):
        for k in range(levels - 1):
            up[k, c] = tok_up(k, c)
        own[c] = tok_own(c)
    for c in range(early):
        for k in range(levels - 1):
            up[k, c].wait_recv()
            side[k, c] = tok_side(k, c)
    for h, i in pieces[first:]:
        att.softmaxes(h, i)

    for k in range(spans - 1):
        origin = (x + spans - k - 1) % spans
        wx[k].wait_recv()
        block = wc_block(half, origin * 2 + core)
        wd.append(begin(remote(block, block, wd_s.at[1 + k], wd_r.at[1 + k], me, other)))
    for c in range(early, CHUNKS):
        for k in range(levels - 1):
            up[k, c].wait_recv()
            side[k, c] = tok_side(k, c)
    cots = [
        begin(
            remote(
                cot_ref.at[:, lane(s * feats, feats)],
                coth.at[me],
                c_s.at[k],
                c_r.at[k],
                s,
                dp,
            )
        )
        for k, s in enumerate(sp_peers)
    ]
    locals_[0].wait()

    def turn(b):
        tok_t[:, lane(b * rows, rows)] = tokens[b].astype(F32).T.astype(BF16)

    turn(pos)
    wb[0].wait_recv()
    block = wc_block(1 - half, dp)
    wx2 = [
        begin(remote(block, block, wx_s.at[1, k], wx_r.at[1, k], me, xk * 2 + core))
        for k, xk in enumerate(xs)
    ]
    wd.append(begin(remote(block, block, wd_s.at[spans], wd_r.at[spans], me, other)))
    for k in range(levels - 1):
        turn(((level + levels - k - 1) % levels) * 2 + y)
    for c in range(CHUNKS):
        own[c].wait_recv()
    turn(level * 2 + 1 - y)
    for k in range(spans - 1):
        origin = (x + spans - k - 1) % spans
        wx2[k].wait_recv()
        block = wc_block(1 - half, origin * 2 + core)
        slot = spans + 1 + k
        wd.append(begin(remote(block, block, wd_s.at[slot], wd_r.at[slot], me, other)))
    for copy in wd:
        copy.wait_recv()

    def weight():
        return wc[...].reshape(depth, 2 * feats)

    def values_of(b, k):
        vloc[b] = dot_nn(tokens[b], weight()).astype(BF16)
        copy = begin(
            remote(
                vloc.at[b, :, lane((1 - half) * feats, feats)],
                v_ref.at[half, b],
                v_s.at[k],
                v_r.at[k],
                partner,
                dp,
            )
        )
        v_ref[half, b] = vloc[b, :, lane(half * feats, feats)]
        return copy

    downs = [(level + levels - k - 1) % levels for k in range(levels - 1)]
    v_copies = [values_of(pos, 0)]
    for k in range(levels - 1):
        v_copies.append(values_of(downs[k] * 2 + y, 1 + k))
    v_copies.append(values_of(level * 2 + 1 - y, levels))
    for k in range(levels - 1):
        for c in range(CHUNKS):
            side[k, c].wait_recv()
        b = downs[k] * 2 + 1 - y
        v_copies.append(values_of(b, levels + 1 + k))
    for k in range(levels - 1):
        turn(downs[k] * 2 + 1 - y)
    for copy in v_copies:
        copy.wait_recv()
    locals_[1].wait()
    for copy in cots:
        copy.wait_recv()

    for h in range(heads):
        att.values_grad(h)
        gvb[:, :, :, h * width : (h + 1) * width] = (
            gv_acc[...].astype(BF16).reshape(2, place, rows, width)
        )
    order = (
        [u * 2 + 1 - y for u in ups] + [level * 2 + 1 - y] + [u * 2 + y for u in ups] + [pos]
    )
    dv_copies = [
        begin(
            remote(
                gvb.at[1 - half, b],
                dv.at[b, :, lane(half * feats, feats)],
                dv_s.at[k],
                dv_r.at[k],
                partner,
                dp,
            )
        )
        for k, b in enumerate(order)
    ]
    for b in range(place):
        dv[b, :, lane(half * feats, feats)] = gvb[half, b]
    split = (heads + 1) // 2
    for h in range(split):
        att.scores_grad(h)

    def partial(k):
        dv_copies[k].wait_recv()
        part[order[k]] = dot_nt(dv[order[k]], weight()).astype(BF16)

    ys = {}
    for k in range(levels):
        partial(k)
        slot = k if k < levels - 1 else levels - 1
        for c in range(CHUNKS):
            ys[k, c] = begin(
                remote(
                    part.at[order[k], chunk(c)],
                    ry.at[slot, chunk(c)],
                    y_s.at[slot, c],
                    y_r.at[slot, c],
                    beside,
                    dp,
                )
            )
    for h in range(split, heads):
        att.scores_grad(h)
    for k in range(levels, 2 * levels):
        partial(k)
    ls = [
        begin(remote(gl_ref, lbuf.at[k], l_s.at[k], l_r.at[k], me, d))
        for k, d in enumerate(dp_peers)
    ]

    count = w_ref.shape[0]
    stretch = m * count
    dv_all = dv[...].reshape(place * rows, 2 * feats)
    as_, bs, es, ds_ = {}, {}, {}, {}
    for p in range(place):
        for h in range(2):
            start = (h * place + p) * stretch
            term[h, p] = (
                dot_nn(tok_t[start : start + stretch], dv_all)
                .astype(BF16)
                .reshape(spans, 2, count, 2 * feats)
            )
        as_[p] = begin(
            remote(term.at[:, p, :, 1 - core], ra.at[p], a_s.at[p], a_r.at[p], me, other)
        )
    for p in range(place):
        as_[p].wait_recv()
        sa[p] = (term[:, p, :, core].astype(F32) + ra[p].astype(F32)).astype(BF16)
        for k, xk in enumerate(xs):
            bs[p, k] = begin(
                remote(
                    sa.at[p, :, xk], rb.at[k, p], b_s.at[k, p], b_r.at[k, p], me, xk * 2 + core
                )
            )

    def rows_up(c):
        for k in range(levels - 1):
            ys[k, c].wait_recv()
            total = part[ups[k] * 2 + y, chunk(c)].astype(F32) + ry[k, chunk(c)].astype(F32)
            sz[k, chunk(c)] = total.astype(BF16)
            zs[k, c] = begin(
                remote(
                    sz.at[k, chunk(c)],
                    rz.at[k, chunk(c)],
                    z_s.at[k, c],
                    z_r.at[k, c],
                    at_pos(ups[k] * 2 + y),
                    dp,
                )
            )

    def to_partner(p):
        total = sa[p, :, x].astype(F32)
        for k in range(spans - 1):
            bs[p, k].wait_recv()
            total = total + rb[k, p].astype(F32)
        sb[p] = total.astype(BF16)
        es[p] = begin(remote(sb.at[p, 1 - half], rc.at[p], e_s.at[p], e_r.at[p], partner, dp))

    def finish(p):
        es[p].wait_recv()
        sc[p] = (sb[p, half].astype(F32) + rc[p].astype(F32)).astype(BF16)

    zs = {}
    for i in range(max(place, CHUNKS)):
        if i < CHUNKS:
            rows_up(i)
        if i < place:
            to_partner(i)
        if 0 < i <= place:
            finish(i - 1)
    for i in range(max(place, CHUNKS) - 1, place):
        finish(i)
    for k, p in enumerate(in_half):
        ds_[k] = begin(
            remote(sc.at[p], rd.at[pos], d_s.at[k], d_r.at[k], at_pos(p), dp)
        )
    rd[pos] = sc[pos]
    for c in range(CHUNKS):
        total = part[pos, chunk(c)].astype(F32)
        ys[levels - 1, c].wait_recv()
        total = total + ry[levels - 1, chunk(c)].astype(F32)
        for k in range(levels - 1):
            zs[k, c].wait_recv()
            total = total + rz[k, chunk(c)].astype(F32)
        gt_ref[chunk(c)] = total.astype(BF16)
    lam = gl_ref[...]
    for k in range(m - 1):
        ls[k].wait_recv()
        lam = lam + lbuf[k]
    glo_ref[...] = lam
    for k in range(place - 1):
        ds_[k].wait_recv()
    for p in range(place):
        for j in range(2):
            start = (j * place + p) * feats
            gw_ref[:, start : start + feats] = rd[p, :, j * feats : (j + 1) * feats].astype(F32)
    for copy in done:
        copy.wait_send()


def run(lambdas, tokens, cotangent, weight, queries, keys, n, m, width):
    rows, depth = tokens.shape
    count, features = weight.shape
    length, feats = queries.shape
    heads = feats // width
    place, levels, spans = n // 2, n // 4, m // 2
    block = min(QBLOCK, length)
    blocks = length // block
    tri = block * (blocks * (blocks + 1) // 2)
    vmem = pl.BlockSpec(memory_space=pltpu.VMEM)
    hbm = pl.BlockSpec(memory_space=pltpu.HBM)
    pair = 2 * feats

    def b16(*shape):
        return pltpu.VMEM(shape, BF16)

    def f32(*shape):
        return pltpu.VMEM(shape, F32)

    def dma(*shape):
        return [pltpu.SemaphoreType.DMA(tuple(max(s, 1) for s in shape))] * 2

    return pl.pallas_call(
        functools.partial(whole_kernel, n, m, width),
        out_shape=[
            jax.ShapeDtypeStruct((length, feats), BF16),
            jax.ShapeDtypeStruct((length, feats), BF16),
            jax.ShapeDtypeStruct((rows, depth), BF16),
            jax.ShapeDtypeStruct((count, features), F32),
            jax.ShapeDtypeStruct((heads, 8, 128), F32),
        ],
        in_specs=[pl.BlockSpec(memory_space=pltpu.SMEM), hbm, hbm, hbm, vmem, vmem],
        out_specs=[vmem] * 5,
        scratch_shapes=[
            b16(place, rows, depth),
            b16(depth, place * rows),
            b16(n, m, count, pair),
            b16(n, rows, feats),
            b16(place, rows, pair),
            b16(2, place, rows, feats),
            f32(heads, 2, tri, block),
            b16(heads, tri, block),
            b16(heads, 2, length, width),
            b16(heads, 2, width, length),
            b16(heads, width, length),
            f32(length, width),
            f32(length, width),
            b16(2, place, rows, feats),
            b16(place, rows, pair),
            b16(place, rows, depth),
            b16(levels, rows, depth),
            b16(max(levels - 1, 1), rows, depth),
            b16(max(levels - 1, 1), rows, depth),
            b16(2, place, spans, 2, count, pair),
            b16(place, 2, spans, count, pair),
            b16(place, 2, spans, count, pair),
            b16(max(spans - 1, 1), place, 2, count, pair),
            b16(place, 2, count, pair),
            b16(place, count, pair),
            b16(place, count, pair),
            b16(place, count, pair),
            f32(heads, 8, 128),
            f32(m - 1, heads, 8, 128),
            pltpu.SemaphoreType.DMA((4,)),
        ]
        + dma(place - 1, 2)
        + dma(1)
        + dma(2, spans - 1)
        + dma(2 * spans)
        + dma(levels - 1, CHUNKS)
        + dma(levels, CHUNKS)
        + dma(n - 1)
        + dma(place)
        + dma(place)
        + dma(levels, CHUNKS)
        + dma(levels - 1, CHUNKS)
        + dma(place)
        + dma(spans - 1, place)
        + dma(place)
        + dma(place - 1)
        + dma(m - 1),
        compiler_params=pltpu.CompilerParams(
            collective_id=0, has_side_effects=True, vmem_limit_bytes=60 * 1024 * 1024
        ),
        name="whole",
    )(lambdas, tokens, cotangent, weight, queries, keys)


def body(n, m, tokens, cotangent, value_weight, query_heads, key_heads, lambdas):
    _, length, head_count, width = query_heads.shape
    feats = head_count * width
    grad_query, grad_key, grad_tokens, grad_weight, lambda_sum = run(
        lambdas,
        tokens[0],
        cotangent[0],
        value_weight,
        query_heads.reshape(length, feats),
        key_heads.reshape(length, feats),
        n,
        m,
        width,
    )
    return (
        grad_query.reshape(1, length, head_count, width),
        grad_key.reshape(1, length, head_count, width),
        grad_tokens[None],
        grad_weight,
        lambda_sum[:, 0, 0],
    )


def solution(mesh):
    placed = (
        P("dp", "sp", None),
        P("dp", "sp", None),
        P(("sp", "dp"), None),
        P("dp", None, "sp", None),
        P("dp", None, "sp", None),
        P("sp"),
    )
    return jax.shard_map(
        functools.partial(body, mesh.shape["sp"], mesh.shape["dp"]),
        mesh=mesh,
        in_specs=placed,
        out_specs=(
            P("dp", None, "sp", None),
            P("dp", None, "sp", None),
            P("dp", "sp", None),
            P(("sp", "dp"), None),
            P("sp"),
        ),
        check_vma=False,
    )
```

time: 144 us -> 108 us (0.75)
  Pallas kernels: 128 us -> 98.1 us
  matrix products: 5.81 us -> 0 us
    pallas_call x3 -> x1, Pallas kernels: 128 us -> 98.1 us  [run(): pl.pallas_call(functools.partial(whole_kernel, n, m, width), out_shape=[j...]
    dot_general x3 -> x0, matrix products: 5.81 us -> none  [the longest x1 3.23 us: dot_nt(): lax.dot_general(a, b, (((1,), (1,)), ((), ())), preferred_element_type=F32)]
    unnamed x12 -> x8, local copies, waits for them, and re-layouts: 4.63 us -> 2.2 us
where the time goes in v1:
time: 108 us
  Pallas kernels  98.1 us (91%)
  local copies, waits for them, and re-layouts  8.76 us (8%)
    pallas_call x1, Pallas kernels, run(): pl.pallas_call(functools.partial(whole_kernel, n, m, width), out_shape=[j...  98.1 us
    reshape x1, local copies, waits for them, and re-layouts, body(): key_heads.reshape(length, feats)  2.32 us
    unnamed x8, local copies, waits for them, and re-layouts  2.2 us

profile of v1, /device:TPU:0, one launch (start us, length us, event | category | flops | bytes accessed | tf_op | source)
XLA Modules:
  0.0 107.5 jit_solution(4723061095062766017)
XLA Ops:
  0.6 2.3 %copy_bitcast_fusion = (bf16[1024,256]{1,0:T(8,128)(2,1)}, bf16[1024,256]{1,0:T(8,128)(2,1)}) fusion(bf16[128,8,2,128]{3,2,1,0:T(2,128)(2,1)} %bitcast.14, bf16[128,8,2,128]{3,2,1,0:T(2,128)(2,1)} %bitcast.15), kind=kLoop, calls=%fused_computation | loop fusion | bytes 2097152 | tf_op jit(solution)/shard_map/reshape | solution.py:651
  3.0 98.1 %whole.1 = (bf16[1024,256]{1,0:T(8,128)(2,1)}, bf16[1024,256]{1,0:T(8,128)(2,1)}, bf16[128,2048]{1,0:T(8,128)(2,1)}, f32[64,2048]{1,0:T(8,128)}, f32[2,8,128]{2,1,0:T(8,128)}) custom-call(f32[2]{0:T(128)} %lam_ref.1, bf16[128,2048]{1,0:T(8,128)(2,1)} %bitcast.11, bf16[128,2048]{1,0:T(8,128)(2,1)} %bitcast.12, bf16[64,2048]{1,0:T(8,128)(2,1)} %w_ref.1, ...), custom_call_target="tpu_custom_call" | custom-call | tf_op jit(solution)/shard_map/whole/pallas_call | solution.py:576
  101.1 0.0 copy-start.2
  101.1 2.0 %reshape.24 = bf16[1,1024,2,128]{3,2,1,0:T(2,128)(2,1)} reshape(bf16[1024,256]{1,0:T(8,128)(2,1)} %get-tuple-element.10) | data formatting | bytes 1048576 | tf_op jit(solution)/shard_map/reshape | solution.py:657
  103.1 1.3 %slice_reduce_fusion = f32[2]{0:T(128)} fusion(f32[2,8,128]{2,1,0:T(8,128)} %get-tuple-element.14), kind=kLoop, calls=%fused_computation.2 | loop fusion | bytes 16 | tf_op jit(solution)/shard_map/slice | solution.py:661
  104.4 0.0 copy-done.2
  104.4 0.0 copy-start.1
  104.4 0.9 reshape.25
  105.3 0.2 copy-done.1
  105.5 0.0 copy-start
  105.5 0.8 copy.17
  106.3 0.4 copy-done
  106.7 0.8 copy.18
Async XLA Ops:
  101.1 3.3 %copy-start.2 = (bf16[1024,256]{1,0:T(8,128)(2,1)S(1)}, bf16[1024,256]{1,0:T(8,128)(2,1)}, u32[]{:S(2)}) copy-start(bf16[1024,256]{1,0:T(8,128)(2,1)} %get-tuple-element.11) | copy-start | bytes 1572868
  104.4 1.1 %copy-start.1 = (bf16[128,2048]{1,0:T(8,128)(2,1)S(1)}, bf16[128,2048]{1,0:T(8,128)(2,1)}, u32[]{:S(2)}) copy-start(bf16[128,2048]{1,0:T(8,128)(2,1)} %get-tuple-element.12) | copy-start | bytes 1572868
  105.5 1.2 %copy-start = (f32[64,2048]{1,0:T(8,128)S(1)}, f32[64,2048]{1,0:T(8,128)}, u32[]{:S(2)}) copy-start(f32[64,2048]{1,0:T(8,128)} %get-tuple-element.25) | copy-start | bytes 1572868

commit v2 on v1

--- a/solution.py
+++ b/solution.py
@@ -1,4 +1,5 @@
 import functools
+import math
 
 import jax
 import jax.numpy as jnp
@@ -163,12 +164,13 @@
 
 
 def whole_kernel(
-    n, m, width,
-    lam_ref, tok_ref, cot_ref, w_ref, q_ref, k_ref,
+    n, m,
+    lam_in, tok_ref, cot_ref, w_ref, q_ref, k_ref,
     gq_ref, gk_ref, gt_ref, gw_ref, glo_ref,
+    lam_ref, q_nat, k_nat, qf, kf, gqf, gkf,
     tokens, tok_t, wc, coth, vloc, v_ref, p_ref, a_ref, qh_ref, kt_ref, go_ref, gv_acc, gk_acc,
     gvb, dv, part, ry, sz, rz, term, ra, sa, rb, sb, rc, sc, rd, gl_ref, lbuf,
-    local_sem, wa_s, wa_r, wb_s, wb_r, wx_s, wx_r, wd_s, wd_r, tz_s, tz_r, ty_s, ty_r,
+    local_sem, wa_s, wa_r, wx_s, wx_r, wd_s, wd_r, tz_s, tz_r, ty_s, ty_r,
     c_s, c_r, v_s, v_r, dv_s, dv_r, y_s, y_r, z_s, z_r, a_s, a_r, b_s, b_r, e_s, e_r,
     d_s, d_r, l_s, l_r,
 ):
@@ -180,9 +182,9 @@
     half, pos = me // place, me % place
     level, y = pos // 2, pos % 2
     x, core = dp // 2, dp % 2
-    heads = lam_ref.shape[0]
     rows, depth = tok_ref.shape
-    feats = q_ref.shape[1]
+    length, heads, width = q_ref.shape
+    feats = heads * width
     part_rows = rows // CHUNKS
     partner = (1 - half) * place + pos
     beside = me + 1 - 2 * y
@@ -211,6 +213,10 @@
             local_sem.at[2 + j],
         )
         for j in range(2)
+    ] + [
+        pltpu.make_async_copy(q_ref, q_nat, local_sem.at[4]),
+        pltpu.make_async_copy(k_ref, k_nat, local_sem.at[5]),
+        pltpu.make_async_copy(lam_in, lam_ref, local_sem.at[6]),
     ]
     for copy in locals_:
         copy.start()
@@ -221,20 +227,18 @@
         done.append(copy)
         return copy
 
-    wa = [
-        begin(
+    def weight_out(k, s, j):
+        start = (j * place + s % place) * feats
+        return begin(
             remote(
-                w_ref.at[:, lane((j * place + p) * feats, feats)],
+                w_ref.at[:, lane(start, feats)],
                 wc.at[me, dp, :, pl.ds(j * feats, feats)],
                 wa_s.at[k, j],
                 wa_r.at[k, j],
-                at_pos(p),
+                s,
                 dp,
             )
         )
-        for k, p in enumerate(in_half)
-        for j in range(2)
-    ]
 
     def chunk(c):
         return pl.ds(c * part_rows, part_rows)
@@ -251,43 +255,47 @@
             )
         )
 
-    def tok_own(c):
+    def tok_side(slot, origin, c):
+        src = tok_ref.at[chunk(c)] if slot == 0 else tokens.at[origin, chunk(c)]
         return begin(
             remote(
-                tok_ref.at[chunk(c)],
-                tokens.at[pos, chunk(c)],
-                ty_s.at[0, c],
-                ty_r.at[0, c],
+                src,
+                tokens.at[origin, chunk(c)],
+                ty_s.at[slot, c],
+                ty_r.at[slot, c],
                 beside,
                 dp,
             )
         )
 
-    def tok_side(k, c):
-        origin = ((level + levels - k - 1) % levels) * 2 + y
-        return begin(
-            remote(
-                tokens.at[origin, chunk(c)],
-                tokens.at[origin, chunk(c)],
-                ty_s.at[k + 1, c],
-                ty_r.at[k + 1, c],
-                beside,
-                dp,
-            )
-        )
-
-    up, own, side = {}, {}, {}
-    early = CHUNKS // 2
-    for c in range(early):
+    def cot_out(k, s):
+        return remote(
+            cot_ref.at[:, lane(s * feats, feats)], coth.at[me], c_s.at[k], c_r.at[k], s, dp
+        )
+
+    far = [(1 - half) * place + (pos + k) % place for k in range(place)]
+    near = [at_pos(p) for p in in_half]
+    wa = [weight_out(place + k, s, j) for k, s in enumerate(near) for j in range(2)]
+    wb = [[weight_out(k, s, j) for j in range(2)] for k, s in enumerate(far)]
+    up, side = {}, {}
+    for c in range(CHUNKS):
         for k in range(levels - 1):
             up[k, c] = tok_up(k, c)
-        own[c] = tok_own(c)
-
+    own = [tok_side(0, pos, c) for c in range(CHUNKS)]
+    far_cots = [cot_out(k, s) for k, s in enumerate(far)]
+    near_cots = [cot_out(place + k, s) for k, s in enumerate(near)]
+    done.extend(far_cots + near_cots)
+    for copy in far_cots:
+        copy.start()
     att = Attention(
-        lam_ref, q_ref, k_ref, v_ref, coth,
+        lam_ref, qf, kf, v_ref, coth,
         (p_ref, a_ref, qh_ref, kt_ref, go_ref, gv_acc, gk_acc),
-        (gq_ref, gk_ref, gl_ref), width,
+        (gqf, gkf, gl_ref), width,
     )
+    for copy in locals_[4:]:
+        copy.wait()
+    qf[...] = q_nat[...].reshape(length, feats)
+    kf[...] = k_nat[...].reshape(length, feats)
     pieces = [(h, i) for h in range(heads) for i in range(att.count)]
     for h in range(heads):
         att.prepare(h)
@@ -295,77 +303,74 @@
     for h, i in pieces[:first]:
         att.softmaxes(h, i)
 
-    def wc_block(h, d):
-        return wc.at[pl.ds(h * place, place), d]
-
-    for copy in locals_[2:]:
+    def wc_block(h, p, d):
+        return wc.at[h * place + p, d]
+
+    for copy in locals_[2:4]:
         copy.wait()
     for copy in wa:
         copy.wait_recv()
-    mine = wc_block(half, dp)
-    wb = [begin(remote(mine, mine, wb_s.at[0], wb_r.at[0], partner, dp))]
-    wx = [
-        begin(remote(mine, mine, wx_s.at[0, k], wx_r.at[0, k], me, xk * 2 + core))
-        for k, xk in enumerate(xs)
-    ]
-    wd = [begin(remote(mine, mine, wd_s.at[0], wd_r.at[0], me, other))]
-    for c in range(early, CHUNKS):
-        for k in range(levels - 1):
-            up[k, c] = tok_up(k, c)
-        own[c] = tok_own(c)
-    for c in range(early):
+    wx, wd = {}, []
+
+    def core_out(slot, p, block):
+        wd.append(
+            begin(remote(block, block, wd_s.at[slot, p], wd_r.at[slot, p], me, other))
+        )
+
+    def x_out(j, p, block):
+        for k, xk in enumerate(xs):
+            wx[j, k, p] = begin(
+                remote(
+                    block, block, wx_s.at[j, k, p], wx_r.at[j, k, p], me, xk * 2 + core
+                )
+            )
+
+    for p in range(place):
+        block = wc_block(half, p, dp)
+        x_out(0, p, block)
+        core_out(0, p, block)
+    for h, i in pieces[first:]:
+        att.softmaxes(h, i)
+    downs = [(level + levels - k - 1) % levels for k in range(levels - 1)]
+    x_downs = [(x + spans - k - 1) % spans for k in range(spans - 1)]
+
+    def side_on(c):
         for k in range(levels - 1):
             up[k, c].wait_recv()
-            side[k, c] = tok_side(k, c)
-    for h, i in pieces[first:]:
-        att.softmaxes(h, i)
-
-    for k in range(spans - 1):
-        origin = (x + spans - k - 1) % spans
-        wx[k].wait_recv()
-        block = wc_block(half, origin * 2 + core)
-        wd.append(begin(remote(block, block, wd_s.at[1 + k], wd_r.at[1 + k], me, other)))
-    for c in range(early, CHUNKS):
-        for k in range(levels - 1):
-            up[k, c].wait_recv()
-            side[k, c] = tok_side(k, c)
-    cots = [
-        begin(
-            remote(
-                cot_ref.at[:, lane(s * feats, feats)],
-                coth.at[me],
-                c_s.at[k],
-                c_r.at[k],
-                s,
-                dp,
-            )
-        )
-        for k, s in enumerate(sp_peers)
-    ]
-    locals_[0].wait()
+            side[k, c] = tok_side(k + 1, downs[k] * 2 + y, c)
 
     def turn(b):
         tok_t[:, lane(b * rows, rows)] = tokens[b].astype(F32).T.astype(BF16)
 
-    turn(pos)
-    wb[0].wait_recv()
-    block = wc_block(1 - half, dp)
-    wx2 = [
-        begin(remote(block, block, wx_s.at[1, k], wx_r.at[1, k], me, xk * 2 + core))
-        for k, xk in enumerate(xs)
-    ]
-    wd.append(begin(remote(block, block, wd_s.at[spans], wd_r.at[spans], me, other)))
+    def x_on(j, p):
+        for k, origin in enumerate(x_downs):
+            wx[j, k, p].wait_recv()
+            slot = (1 + k) if j == 0 else (spans + 1 + k)
+            h, q = (half, p) if j == 0 else (1 - half, (pos + place - p) % place)
+            core_out(slot, p, wc_block(h, q, origin * 2 + core))
+
+    for k in range(place):
+        for copy in wb[k]:
+            copy.wait_recv()
+        block = wc_block(1 - half, (pos + place - k) % place, dp)
+        x_out(1, k, block)
+        core_out(spans, k, block)
+    for p in range(place):
+        x_on(0, p)
+    locals_[0].wait()
+    for c in range(CHUNKS):
+        side_on(c)
+        if c == 0:
+            turn(pos)
+    for copy in near_cots:
+        copy.start()
     for k in range(levels - 1):
-        turn(((level + levels - k - 1) % levels) * 2 + y)
-    for c in range(CHUNKS):
-        own[c].wait_recv()
+        turn(downs[k] * 2 + y)
+    for copy in own:
+        copy.wait_recv()
     turn(level * 2 + 1 - y)
-    for k in range(spans - 1):
-        origin = (x + spans - k - 1) % spans
-        wx2[k].wait_recv()
-        block = wc_block(1 - half, origin * 2 + core)
-        slot = spans + 1 + k
-        wd.append(begin(remote(block, block, wd_s.at[slot], wd_r.at[slot], me, other)))
+    for p in range(place):
+        x_on(1, p)
     for copy in wd:
         copy.wait_recv()
 
@@ -387,7 +392,6 @@
         v_ref[half, b] = vloc[b, :, lane(half * feats, feats)]
         return copy
 
-    downs = [(level + levels - k - 1) % levels for k in range(levels - 1)]
     v_copies = [values_of(pos, 0)]
     for k in range(levels - 1):
         v_copies.append(values_of(downs[k] * 2 + y, 1 + k))
@@ -395,93 +399,96 @@
     for k in range(levels - 1):
         for c in range(CHUNKS):
             side[k, c].wait_recv()
-        b = downs[k] * 2 + 1 - y
-        v_copies.append(values_of(b, levels + 1 + k))
+        v_copies.append(values_of(downs[k] * 2 + 1 - y, levels + 1 + k))
+
     for k in range(levels - 1):
         turn(downs[k] * 2 + 1 - y)
     for copy in v_copies:
         copy.wait_recv()
     locals_[1].wait()
-    for copy in cots:
+    for copy in near_cots + far_cots:
         copy.wait_recv()
 
-    for h in range(heads):
-        att.values_grad(h)
-        gvb[:, :, :, h * width : (h + 1) * width] = (
-            gv_acc[...].astype(BF16).reshape(2, place, rows, width)
-        )
     order = (
         [u * 2 + 1 - y for u in ups] + [level * 2 + 1 - y] + [u * 2 + y for u in ups] + [pos]
     )
-    dv_copies = [
-        begin(
-            remote(
-                gvb.at[1 - half, b],
-                dv.at[b, :, lane(half * feats, feats)],
-                dv_s.at[k],
-                dv_r.at[k],
-                partner,
-                dp,
-            )
-        )
-        for k, b in enumerate(order)
-    ]
-    for b in range(place):
-        dv[b, :, lane(half * feats, feats)] = gvb[half, b]
+    dv_copies = {}
+    for h in range(heads):
+        att.values_grad(h)
+        gvb[h] = gv_acc[...].astype(BF16).reshape(2, place, rows, width)
+        for k, b in enumerate(order):
+            dv_copies[h, k] = begin(
+                remote(
+                    gvb.at[h, 1 - half, b],
+                    dv.at[b, :, lane(half * feats + h * width, width)],
+                    dv_s.at[h, k],
+                    dv_r.at[h, k],
+                    partner,
+                    dp,
+                )
+            )
+        for b in range(place):
+            dv[b, :, lane(half * feats + h * width, width)] = gvb[h, half, b]
     split = (heads + 1) // 2
     for h in range(split):
         att.scores_grad(h)
 
+    def dv_wait(k):
+        for h in range(heads):
+            dv_copies[h, k].wait_recv()
+
     def partial(k):
-        dv_copies[k].wait_recv()
         part[order[k]] = dot_nt(dv[order[k]], weight()).astype(BF16)
 
-    ys = {}
+    ys, zs = {}, {}
     for k in range(levels):
+        dv_wait(k)
         partial(k)
-        slot = k if k < levels - 1 else levels - 1
         for c in range(CHUNKS):
             ys[k, c] = begin(
                 remote(
                     part.at[order[k], chunk(c)],
-                    ry.at[slot, chunk(c)],
-                    y_s.at[slot, c],
-                    y_r.at[slot, c],
+                    ry.at[k, chunk(c)],
+                    y_s.at[k, c],
+                    y_r.at[k, c],
                     beside,
                     dp,
                 )
             )
     for h in range(split, heads):
         att.scores_grad(h)
-    for k in range(levels, 2 * levels):
-        partial(k)
     ls = [
         begin(remote(gl_ref, lbuf.at[k], l_s.at[k], l_r.at[k], me, d))
         for k, d in enumerate(dp_peers)
     ]
+    for k in range(levels, 2 * levels):
+        dv_wait(k)
 
     count = w_ref.shape[0]
     stretch = m * count
     dv_all = dv[...].reshape(place * rows, 2 * feats)
     as_, bs, es, ds_ = {}, {}, {}, {}
-    for p in range(place):
+    turns = in_half + [pos]
+    for k, p in enumerate(turns):
         for h in range(2):
-            start = (h * place + p) * stretch
+            start = pl.multiple_of((h * place + p) * stretch, stretch)
             term[h, p] = (
-                dot_nn(tok_t[start : start + stretch], dv_all)
+                dot_nn(tok_t[pl.ds(start, stretch), :], dv_all)
                 .astype(BF16)
                 .reshape(spans, 2, count, 2 * feats)
             )
-        as_[p] = begin(
-            remote(term.at[:, p, :, 1 - core], ra.at[p], a_s.at[p], a_r.at[p], me, other)
-        )
-    for p in range(place):
-        as_[p].wait_recv()
+        as_[k] = begin(
+            remote(term.at[:, p, :, 1 - core], ra.at[p], a_s.at[k], a_r.at[k], me, other)
+        )
+    for k in range(levels, 2 * levels):
+        partial(k)
+    for k, p in enumerate(turns):
+        as_[k].wait_recv()
         sa[p] = (term[:, p, :, core].astype(F32) + ra[p].astype(F32)).astype(BF16)
-        for k, xk in enumerate(xs):
-            bs[p, k] = begin(
+        for j, xk in enumerate(xs):
+            bs[k, j] = begin(
                 remote(
-                    sa.at[p, :, xk], rb.at[k, p], b_s.at[k, p], b_r.at[k, p], me, xk * 2 + core
+                    sa.at[p, :, xk], rb.at[j, p], b_s.at[j, k], b_r.at[j, k], me, xk * 2 + core
                 )
             )
 
@@ -501,33 +508,36 @@
                 )
             )
 
-    def to_partner(p):
+    def to_partner(k):
+        p = turns[k]
         total = sa[p, :, x].astype(F32)
-        for k in range(spans - 1):
-            bs[p, k].wait_recv()
-            total = total + rb[k, p].astype(F32)
+        for j in range(spans - 1):
+            bs[k, j].wait_recv()
+            total = total + rb[j, p].astype(F32)
         sb[p] = total.astype(BF16)
-        es[p] = begin(remote(sb.at[p, 1 - half], rc.at[p], e_s.at[p], e_r.at[p], partner, dp))
-
-    def finish(p):
-        es[p].wait_recv()
-        sc[p] = (sb[p, half].astype(F32) + rc[p].astype(F32)).astype(BF16)
-
-    zs = {}
-    for i in range(max(place, CHUNKS)):
-        if i < CHUNKS:
-            rows_up(i)
-        if i < place:
-            to_partner(i)
-        if 0 < i <= place:
-            finish(i - 1)
-    for i in range(max(place, CHUNKS) - 1, place):
-        finish(i)
-    for k, p in enumerate(in_half):
-        ds_[k] = begin(
-            remote(sc.at[p], rd.at[pos], d_s.at[k], d_r.at[k], at_pos(p), dp)
-        )
-    rd[pos] = sc[pos]
+        es[k] = begin(remote(sb.at[p, 1 - half], rc.at[p], e_s.at[k], e_r.at[k], partner, dp))
+
+    def finish(k):
+        p = turns[k]
+        es[k].wait_recv()
+        total = (sb[p, half].astype(F32) + rc[p].astype(F32)).astype(BF16)
+        if k < place - 1:
+            sc[p] = total
+            ds_[k] = begin(
+                remote(sc.at[p], rd.at[pos], d_s.at[k], d_r.at[k], at_pos(p), dp)
+            )
+        else:
+            rd[pos] = total
+
+    for c in range(CHUNKS):
+        rows_up(c)
+    gq_ref[...] = gqf[...].reshape(gq_ref.shape)
+    gk_ref[...] = gkf[...].reshape(gk_ref.shape)
+    for k in range(place):
+        to_partner(k)
+        if k > 0:
+            finish(k - 1)
+    finish(place - 1)
     for c in range(CHUNKS):
         total = part[pos, chunk(c)].astype(F32)
         ys[levels - 1, c].wait_recv()
@@ -551,11 +561,41 @@
         copy.wait_send()
 
 
-def run(lambdas, tokens, cotangent, weight, queries, keys, n, m, width):
+def finish_kernel(gq_ref, gk_ref, gt_ref, gw_ref, gl_ref, *refs):
+    outs, lam_out, sems = refs[:4], refs[4], refs[5]
+    copies = [
+        pltpu.make_async_copy(src, dst, sems.at[i])
+        for i, (src, dst) in enumerate(zip((gq_ref, gk_ref, gt_ref, gw_ref), outs))
+    ]
+    for copy in copies:
+        copy.start()
+    for h in range(gl_ref.shape[0]):
+        lam_out[h] = jnp.max(gl_ref[h])
+    for copy in copies:
+        copy.wait()
+
+
+def finish(gq, gk, gt, gw, gl):
+    vmem = pl.BlockSpec(memory_space=pltpu.VMEM)
+    hbm = pl.BlockSpec(memory_space=pltpu.HBM)
+    results = [gq, gk, gt, gw]
+    return pl.pallas_call(
+        finish_kernel,
+        out_shape=[jax.ShapeDtypeStruct(a.shape, a.dtype) for a in results]
+        + [jax.ShapeDtypeStruct(gl.shape[:1], F32)],
+        in_specs=[vmem] * 5,
+        out_specs=[hbm] * 4 + [pl.BlockSpec(memory_space=pltpu.SMEM)],
+        scratch_shapes=[pltpu.SemaphoreType.DMA((4,))],
+        compiler_params=pltpu.CompilerParams(vmem_limit_bytes=2 * 1024 * 1024),
+        name="finish",
+    )(*results, gl)
+
+
+def run(lambdas, tokens, cotangent, weight, queries, keys, n, m):
     rows, depth = tokens.shape
     count, features = weight.shape
-    length, feats = queries.shape
-    heads = feats // width
+    length, heads, width = queries.shape
+    feats = heads * width
     place, levels, spans = n // 2, n // 4, m // 2
     block = min(QBLOCK, length)
     blocks = length // block
@@ -573,18 +613,15 @@
     def dma(*shape):
         return [pltpu.SemaphoreType.DMA(tuple(max(s, 1) for s in shape))] * 2
 
-    return pl.pallas_call(
-        functools.partial(whole_kernel, n, m, width),
-        out_shape=[
-            jax.ShapeDtypeStruct((length, feats), BF16),
-            jax.ShapeDtypeStruct((length, feats), BF16),
-            jax.ShapeDtypeStruct((rows, depth), BF16),
-            jax.ShapeDtypeStruct((count, features), F32),
-            jax.ShapeDtypeStruct((heads, 8, 128), F32),
-        ],
-        in_specs=[pl.BlockSpec(memory_space=pltpu.SMEM), hbm, hbm, hbm, vmem, vmem],
-        out_specs=[vmem] * 5,
-        scratch_shapes=[
+    scratch = (
+        [
+            pltpu.SMEM((heads,), F32),
+            b16(length, heads, width),
+            b16(length, heads, width),
+            b16(length, feats),
+            b16(length, feats),
+            b16(length, feats),
+            b16(length, feats),
             b16(place, rows, depth),
             b16(depth, place * rows),
             b16(n, m, count, pair),
@@ -598,7 +635,7 @@
             b16(heads, width, length),
             f32(length, width),
             f32(length, width),
-            b16(2, place, rows, feats),
+            b16(heads, 2, place, rows, width),
             b16(place, rows, pair),
             b16(place, rows, depth),
             b16(levels, rows, depth),
@@ -614,52 +651,58 @@
             b16(place, count, pair),
             f32(heads, 8, 128),
             f32(m - 1, heads, 8, 128),
-            pltpu.SemaphoreType.DMA((4,)),
+            pltpu.SemaphoreType.DMA((7,)),
         ]
-        + dma(place - 1, 2)
-        + dma(1)
-        + dma(2, spans - 1)
-        + dma(2 * spans)
+        + dma(n - 1, 2)
+        + dma(2, spans - 1, place)
+        + dma(2 * spans, place)
         + dma(levels - 1, CHUNKS)
         + dma(levels, CHUNKS)
         + dma(n - 1)
         + dma(place)
-        + dma(place)
+        + dma(heads, place)
         + dma(levels, CHUNKS)
         + dma(levels - 1, CHUNKS)
         + dma(place)
         + dma(spans - 1, place)
         + dma(place)
         + dma(place - 1)
-        + dma(m - 1),
+        + dma(m - 1)
+    )
+    held = sum(
+        math.prod(ref.shape) * jnp.dtype(ref.dtype).itemsize
+        for ref in scratch
+        if ref.memory_space == pltpu.VMEM
+    )
+    return pl.pallas_call(
+        functools.partial(whole_kernel, n, m),
+        out_shape=[
+            jax.ShapeDtypeStruct((length, heads, width), BF16),
+            jax.ShapeDtypeStruct((length, heads, width), BF16),
+            jax.ShapeDtypeStruct((rows, depth), BF16),
+            jax.ShapeDtypeStruct((count, features), F32),
+            jax.ShapeDtypeStruct((heads, 8, 128), F32),
+        ],
+        in_specs=[pl.BlockSpec(memory_space=pltpu.HBM if heads > 1 else pl.ANY), hbm, hbm, hbm, hbm, hbm],
+        out_specs=[vmem] * 5,
+        scratch_shapes=scratch,
         compiler_params=pltpu.CompilerParams(
-            collective_id=0, has_side_effects=True, vmem_limit_bytes=60 * 1024 * 1024
+            collective_id=0, has_side_effects=True, vmem_limit_bytes=held + 8 * 1024 * 1024
         ),
         name="whole",
     )(lambdas, tokens, cotangent, weight, queries, keys)
 
 
 def body(n, m, tokens, cotangent, value_weight, query_heads, key_heads, lambdas):
-    _, length, head_count, width = query_heads.shape
-    feats = head_count * width
-    grad_query, grad_key, grad_tokens, grad_weight, lambda_sum = run(
-        lambdas,
-        tokens[0],
-        cotangent[0],
-        value_weight,
-        query_heads.reshape(length, feats),
-        key_heads.reshape(length, feats),
-        n,
-        m,
-        width,
-    )
-    return (
-        grad_query.reshape(1, length, head_count, width),
-        grad_key.reshape(1, length, head_count, width),
-        grad_tokens[None],
-        grad_weight,
-        lambda_sum[:, 0, 0],
-    )
+    large = [tokens[0], cotangent[0], value_weight, query_heads[0], key_heads[0]]
+    if lambdas.size > 1:
+        large = [lambdas] + large
+    large = [pltpu.with_memory_space_constraint(a, pltpu.HBM) for a in large]
+    if lambdas.size == 1:
+        large = [lambdas] + large
+    results = run(*large, n, m)
+    grad_query, grad_key, grad_tokens, grad_weight, grad_lambda = finish(*results)
+    return grad_query[None], grad_key[None], grad_tokens[None], grad_weight, grad_lambda
 
 
 def solution(mesh):

time: 108 us -> 92.6 us (0.86)
  local copies, waits for them, and re-layouts: 8.76 us -> 0 us
  Pallas kernels: 98.1 us -> 91.6 us
    pallas_call x1 -> x2, Pallas kernels: 98.1 us -> 91.6 us  [the longest x1 89.8 us: run(): pl.pallas_call(functools.partial(whole_kernel, n, m), out_shape=[jax.Shap...]
    reshape x3 -> x0, local copies, waits for them, and re-layouts: 5.26 us -> none  [the longest x1 2.32 us: body(): key_heads.reshape(length, feats)]
    unnamed x8 -> x0, local copies, waits for them, and re-layouts: 2.2 us -> none
    slice x1 -> x0, local copies, waits for them, and re-layouts: 1.31 us -> none  [body(): lambda_sum[:, 0, 0]]
where the time goes in v2:
time: 92.6 us; the launch traced here: 92.4 us
  Pallas kernels  91.6 us (99%)
    pallas_call x1, Pallas kernels, run(): pl.pallas_call(functools.partial(whole_kernel, n, m), out_shape=[jax.Shap...  89.8 us
    pallas_call x1, Pallas kernels, finish(): pl.pallas_call(finish_kernel, out_shape=[jax.ShapeDtypeStruct(a.shape, a....  1.86 us

profile of v2, /device:TPU:0, one launch (start us, length us, event | category | flops | bytes accessed | tf_op | source)
XLA Modules:
  0.0 92.4 jit_solution(1608046857719070322)
XLA Ops:
  0.6 89.8 %whole.1 = (bf16[1024,2,128]{2,1,0:T(2,128)(2,1)S(1)}, bf16[1024,2,128]{2,1,0:T(2,128)(2,1)S(1)}, bf16[128,2048]{1,0:T(8,128)(2,1)S(1)}, f32[64,2048]{1,0:T(8,128)S(1)}, f32[2,8,128]{2,1,0:T(8,128)S(1)}) custom-call(f32[2]{0:T(128)} %lam_in.1, bf16[128,2048]{1,0:T(8,128)(2,1)} %bitcast.7, bf16[128,2048]{1,0:T(8,128)(2,1)} %bitcast.8, ...), custom_call_target="tpu_custom_call" | custom-call | tf_op jit(solution)/shard_map/whole/pallas_call | solution.py:677
  90.4 1.9 %finish.1 = (bf16[1024,2,128]{2,1,0:T(2,128)(2,1)}, bf16[1024,2,128]{2,1,0:T(2,128)(2,1)}, bf16[128,2048]{1,0:T(8,128)(2,1)}, f32[64,2048]{1,0:T(8,128)}, f32[2]{0:T(128)}) custom-call(bf16[1024,2,128]{2,1,0:T(2,128)(2,1)S(1)} %get-tuple-element.15.gq_ref, bf16[1024,2,128]{2,1,0:T(2,128)(2,1)S(1)} %get-tuple-element.16.gk_ref, ...), custom_call_target="tpu_custom_call" | custom-call | tf_op jit(solution)/shard_map/finish/pallas_call | solution.py:582

commit v3 on v2

--- a/solution.py
+++ b/solution.py
@@ -35,12 +35,14 @@
     )
 
 
-def greet(peers):
+def greet(peers, copies):
     barrier = pltpu.get_barrier_semaphore()
     for sp, dp in peers:
         pl.semaphore_signal(
             barrier, inc=1, device_id=(sp, dp), device_id_type=pl.DeviceIdType.MESH
         )
+    for copy in copies:
+        copy.start()
     pl.semaphore_wait(barrier, len(peers))
 
 
@@ -123,12 +125,14 @@
                 self.gv_acc[0:off] += gv[0:off]
             self.gv_acc[off:reach] = gv[off:reach]
 
-    def scores_grad(self, head):
+    def scores_grad(self, head, midway=None):
         block, width = self.block, self.width
         lam = self.lam_ref[head]
         v_all = self.v_ref[:, :, :, self.columns(head)].reshape(self.length, width)
         lambda_total = jnp.zeros((1, block), F32)
         for index in range(self.count):
+            if midway and index == self.count - 1:
+                midway()
             off, reach, pieces, base = self.span(index)
             grad_out = self.go_ref[head, :, off:reach]
             probs = [
@@ -169,9 +173,9 @@
     gq_ref, gk_ref, gt_ref, gw_ref, glo_ref,
     lam_ref, q_nat, k_nat, qf, kf, gqf, gkf,
     tokens, tok_t, wc, coth, vloc, v_ref, p_ref, a_ref, qh_ref, kt_ref, go_ref, gv_acc, gk_acc,
-    gvb, dv, part, ry, sz, rz, term, ra, sa, rb, sb, rc, sc, rd, gl_ref, lbuf,
+    gvb, dv, part, ry, sz, rz, rzd, tokx, acc, sb, rc, sc, rd, gl_ref, lbuf,
     local_sem, wa_s, wa_r, wx_s, wx_r, wd_s, wd_r, tz_s, tz_r, ty_s, ty_r,
-    c_s, c_r, v_s, v_r, dv_s, dv_r, y_s, y_r, z_s, z_r, a_s, a_r, b_s, b_r, e_s, e_r,
+    c_s, c_r, v_s, v_r, dv_s, dv_r, y_s, y_r, z_s, z_r, zd_s, zd_r, tx_s, tx_r, gx_s, gx_r, gd_s, gd_r, e_s, e_r,
     d_s, d_r, l_s, l_r,
 ):
     me = lax.axis_index("sp")
@@ -218,9 +222,7 @@
         pltpu.make_async_copy(k_ref, k_nat, local_sem.at[5]),
         pltpu.make_async_copy(lam_in, lam_ref, local_sem.at[6]),
     ]
-    for copy in locals_:
-        copy.start()
-    greet([(s, dp) for s in sp_peers] + [(me, d) for d in dp_peers])
+    greet([(s, dp) for s in sp_peers] + [(me, d) for d in dp_peers], locals_)
 
     def begin(copy):
         copy.start()
@@ -270,8 +272,11 @@
 
     def cot_out(k, s):
         return remote(
-            cot_ref.at[:, lane(s * feats, feats)], coth.at[me], c_s.at[k], c_r.at[k], s, dp
-        )
+            cot_ref.at[:, lane(s * feats, feats)], coth.at[me], c_s.at[k], c_r.at[me], s, dp
+        )
+
+    def cot_in(s):
+        return remote(coth.at[s], coth.at[s], c_s.at[0], c_r.at[s], s, dp)
 
     far = [(1 - half) * place + (pos + k) % place for k in range(place)]
     near = [at_pos(p) for p in in_half]
@@ -282,7 +287,16 @@
         for k in range(levels - 1):
             up[k, c] = tok_up(k, c)
     own = [tok_side(0, pos, c) for c in range(CHUNKS)]
-    far_cots = [cot_out(k, s) for k, s in enumerate(far)]
+    far_cots = [
+        cot_out(
+            2 * j + i,
+            (1 - half) * place
+            + (j + half * (levels - 1 - 2 * j)) * 2
+            + (y if i == 0 else 1 - y),
+        )
+        for j in range(levels)
+        for i in range(2)
+    ]
     near_cots = [cot_out(place + k, s) for k, s in enumerate(near)]
     done.extend(far_cots + near_cots)
     for copy in far_cots:
@@ -339,8 +353,27 @@
             up[k, c].wait_recv()
             side[k, c] = tok_side(k + 1, downs[k] * 2 + y, c)
 
-    def turn(b):
-        tok_t[:, lane(b * rows, rows)] = tokens[b].astype(F32).T.astype(BF16)
+    count = w_ref.shape[0]
+    txs = {}
+
+    def turn(slot, b):
+        turned = tokens[b].astype(F32).T.astype(BF16).reshape(2, place, m, count, rows)
+        for h in range(2):
+            for p in range(place):
+                tok_t[b, p, h] = turned[h, p]
+        stretch = lane((dp * place + b) * rows, rows)
+        for k, d in enumerate(dp_peers):
+            txs[k, slot] = begin(
+                remote(
+                    tok_t.at[b, :, :, d],
+                    tokx.at[:, :, :, stretch],
+                    tx_s.at[k, slot],
+                    tx_r.at[k, slot],
+                    me,
+                    d,
+                )
+            )
+        tokx[:, :, :, stretch] = tok_t[b, :, :, dp]
 
     def x_on(j, p):
         for k, origin in enumerate(x_downs):
@@ -361,16 +394,17 @@
     for c in range(CHUNKS):
         side_on(c)
         if c == 0:
-            turn(pos)
+            turn(0, pos)
+        if c == CHUNKS // 2 - 1:
+            for p in range(place):
+                x_on(1, p)
     for copy in near_cots:
         copy.start()
     for k in range(levels - 1):
-        turn(downs[k] * 2 + y)
+        turn(1 + k, downs[k] * 2 + y)
     for copy in own:
         copy.wait_recv()
-    turn(level * 2 + 1 - y)
-    for p in range(place):
-        x_on(1, p)
+    turn(levels, level * 2 + 1 - y)
     for copy in wd:
         copy.wait_recv()
 
@@ -402,56 +436,123 @@
         v_copies.append(values_of(downs[k] * 2 + 1 - y, levels + 1 + k))
 
     for k in range(levels - 1):
-        turn(downs[k] * 2 + 1 - y)
+        turn(levels + 1 + k, downs[k] * 2 + 1 - y)
     for copy in v_copies:
         copy.wait_recv()
     locals_[1].wait()
-    for copy in near_cots + far_cots:
-        copy.wait_recv()
+    for s in sp_peers:
+        cot_in(s).wait_recv()
 
     order = (
         [u * 2 + 1 - y for u in ups] + [level * 2 + 1 - y] + [u * 2 + y for u in ups] + [pos]
     )
     dv_copies = {}
+
+    def dv_out(h, k):
+        dv_copies[h, k] = begin(
+            remote(
+                gvb.at[h, 1 - half, order[k]],
+                dv.at[dp, order[k], :, lane(half * feats + h * width, width)],
+                dv_s.at[h, k],
+                dv_r.at[h, k],
+                partner,
+                dp,
+            )
+        )
+
     for h in range(heads):
         att.values_grad(h)
         gvb[h] = gv_acc[...].astype(BF16).reshape(2, place, rows, width)
-        for k, b in enumerate(order):
-            dv_copies[h, k] = begin(
+        dv_out(h, 0)
+        for b in range(place):
+            dv[dp, b, :, lane(half * feats + h * width, width)] = gvb[h, half, b]
+
+    gxs, gds = {}, []
+
+    def share(d, j):
+        if j == 0:
+            return dv.at[d, :, :, lane(half * feats, feats)]
+        return dv.at[d, order[j - 1], :, lane((1 - half) * feats, feats)]
+
+    def share_core(slot, j, d):
+        gds.append(
+            begin(
                 remote(
-                    gvb.at[h, 1 - half, b],
-                    dv.at[b, :, lane(half * feats + h * width, width)],
-                    dv_s.at[h, k],
-                    dv_r.at[h, k],
-                    partner,
-                    dp,
+                    share(d, j), share(d, j), gd_s.at[slot, j], gd_r.at[slot, j], me, other
                 )
             )
-        for b in range(place):
-            dv[b, :, lane(half * feats + h * width, width)] = gvb[h, half, b]
+        )
+
+    def share_out(j):
+        for k, xk in enumerate(xs):
+            gxs[k, j] = begin(
+                remote(
+                    share(dp, j),
+                    share(dp, j),
+                    gx_s.at[k, j],
+                    gx_r.at[k, j],
+                    me,
+                    xk * 2 + core,
+                )
+            )
+        share_core(0, j, dp)
+
+    def share_on(j):
+        for k, origin in enumerate(x_downs):
+            gxs[k, j].wait_recv()
+            share_core(1 + k, j, origin * 2 + core)
+
+    share_out(0)
     split = (heads + 1) // 2
+
+    def dv_more():
+        for h in range(heads):
+            for k in range(1, levels):
+                dv_out(h, k)
+
     for h in range(split):
-        att.scores_grad(h)
+        att.scores_grad(h, dv_more if h == 0 else None)
 
     def dv_wait(k):
         for h in range(heads):
             dv_copies[h, k].wait_recv()
+        share_out(1 + k)
 
     def partial(k):
-        part[order[k]] = dot_nt(dv[order[k]], weight()).astype(BF16)
-
-    ys, zs = {}, {}
+        part[order[k]] = dot_nt(dv[dp, order[k]], weight()).astype(BF16)
+
+    ys, zs, zd = {}, {}, {}
+    last = CHUNKS - 1
+
+    def y_out(k, c):
+        ys[k, c] = begin(
+            remote(
+                part.at[order[k], chunk(c)],
+                ry.at[k, chunk(c)],
+                y_s.at[k, c],
+                y_r.at[k, c],
+                beside,
+                dp,
+            )
+        )
+
     for k in range(levels):
         dv_wait(k)
+        if k == 0:
+            for h in range(heads):
+                for j in range(levels, 2 * levels):
+                    dv_out(h, j)
         partial(k)
-        for c in range(CHUNKS):
-            ys[k, c] = begin(
+        for c in range(last):
+            y_out(k, c)
+        if k < levels - 1:
+            zd[k] = begin(
                 remote(
-                    part.at[order[k], chunk(c)],
-                    ry.at[k, chunk(c)],
-                    y_s.at[k, c],
-                    y_r.at[k, c],
-                    beside,
+                    part.at[order[k], chunk(last)],
+                    rzd.at[k],
+                    zd_s.at[k],
+                    zd_r.at[k],
+                    at_pos(ups[k] * 2 + y),
                     dp,
                 )
             )
@@ -461,41 +562,20 @@
         begin(remote(gl_ref, lbuf.at[k], l_s.at[k], l_r.at[k], me, d))
         for k, d in enumerate(dp_peers)
     ]
-    for k in range(levels, 2 * levels):
-        dv_wait(k)
-
-    count = w_ref.shape[0]
-    stretch = m * count
-    dv_all = dv[...].reshape(place * rows, 2 * feats)
-    as_, bs, es, ds_ = {}, {}, {}, {}
-    turns = in_half + [pos]
-    for k, p in enumerate(turns):
-        for h in range(2):
-            start = pl.multiple_of((h * place + p) * stretch, stretch)
-            term[h, p] = (
-                dot_nn(tok_t[pl.ds(start, stretch), :], dv_all)
-                .astype(BF16)
-                .reshape(spans, 2, count, 2 * feats)
-            )
-        as_[k] = begin(
-            remote(term.at[:, p, :, 1 - core], ra.at[p], a_s.at[k], a_r.at[k], me, other)
-        )
-    for k in range(levels, 2 * levels):
-        partial(k)
-    for k, p in enumerate(turns):
-        as_[k].wait_recv()
-        sa[p] = (term[:, p, :, core].astype(F32) + ra[p].astype(F32)).astype(BF16)
-        for j, xk in enumerate(xs):
-            bs[k, j] = begin(
-                remote(
-                    sa.at[p, :, xk], rb.at[j, p], b_s.at[j, k], b_r.at[j, k], me, xk * 2 + core
-                )
-            )
+    def last_out():
+        total = part[order[levels - 1], chunk(last)].astype(F32)
+        for k in range(levels - 1):
+            zd[k].wait_recv()
+            total = total + rzd[k].astype(F32)
+        part[order[levels - 1], chunk(last)] = total.astype(BF16)
+        y_out(levels - 1, last)
 
     def rows_up(c):
         for k in range(levels - 1):
-            ys[k, c].wait_recv()
-            total = part[ups[k] * 2 + y, chunk(c)].astype(F32) + ry[k, chunk(c)].astype(F32)
+            total = part[ups[k] * 2 + y, chunk(c)].astype(F32)
+            if c < last:
+                ys[k, c].wait_recv()
+                total = total + ry[k, chunk(c)].astype(F32)
             sz[k, chunk(c)] = total.astype(BF16)
             zs[k, c] = begin(
                 remote(
@@ -508,19 +588,40 @@
                 )
             )
 
-    def to_partner(k):
-        p = turns[k]
-        total = sa[p, :, x].astype(F32)
-        for j in range(spans - 1):
-            bs[k, j].wait_recv()
-            total = total + rb[j, p].astype(F32)
-        sb[p] = total.astype(BF16)
-        es[k] = begin(remote(sb.at[p, 1 - half], rc.at[p], e_s.at[k], e_r.at[k], partner, dp))
+    for k in range(levels, 2 * levels - 1):
+        dv_wait(k)
+        partial(k)
+    rows_up(last)
+    rows_up(0)
+    last_out()
+    dv_wait(2 * levels - 1)
+    for j in range(place):
+        share_on(j)
+    for c in range(1, last - 1):
+        rows_up(c)
+    share_on(place)
+    for k in range(m - 1):
+        for slot in range(place):
+            txs[k, slot].wait_recv()
+    for copy in gds:
+        copy.wait_recv()
+
+    es, ds_ = {}, {}
+    turns = in_half + [pos]
+    dv_all = dv[...].reshape(m * place * rows, 2 * feats)
+    for k, p in enumerate(turns):
+        acc[p] = dot_nn(tokx[p].reshape(2 * count, m * place * rows), dv_all).reshape(
+            2, count, 2 * feats
+        )
+        sb[p] = acc[p, 1 - half].astype(BF16)
+        es[k] = begin(remote(sb.at[p], rc.at[p], e_s.at[k], e_r.at[k], partner, dp))
+    rows_up(last - 1)
+    partial(2 * levels - 1)
 
     def finish(k):
         p = turns[k]
         es[k].wait_recv()
-        total = (sb[p, half].astype(F32) + rc[p].astype(F32)).astype(BF16)
+        total = (acc[p, half] + rc[p].astype(F32)).astype(BF16)
         if k < place - 1:
             sc[p] = total
             ds_[k] = begin(
@@ -529,15 +630,10 @@
         else:
             rd[pos] = total
 
-    for c in range(CHUNKS):
-        rows_up(c)
     gq_ref[...] = gqf[...].reshape(gq_ref.shape)
     gk_ref[...] = gkf[...].reshape(gk_ref.shape)
     for k in range(place):
-        to_partner(k)
-        if k > 0:
-            finish(k - 1)
-    finish(place - 1)
+        finish(k)
     for c in range(CHUNKS):
         total = part[pos, chunk(c)].astype(F32)
         ys[levels - 1, c].wait_recv()
@@ -623,7 +719,7 @@
             b16(length, feats),
             b16(length, feats),
             b16(place, rows, depth),
-            b16(depth, place * rows),
+            b16(place, place, 2, m, count, rows),
             b16(n, m, count, pair),
             b16(n, rows, feats),
             b16(place, rows, pair),
@@ -636,16 +732,15 @@
             f32(length, width),
             f32(length, width),
             b16(heads, 2, place, rows, width),
-            b16(place, rows, pair),
+            b16(m, place, rows, pair),
             b16(place, rows, depth),
             b16(levels, rows, depth),
             b16(max(levels - 1, 1), rows, depth),
             b16(max(levels - 1, 1), rows, depth),
-            b16(2, place, spans, 2, count, pair),
-            b16(place, 2, spans, count, pair),
-            b16(place, 2, spans, count, pair),
-            b16(max(spans - 1, 1), place, 2, count, pair),
-            b16(place, 2, count, pair),
+            b16(max(levels - 1, 1), rows // CHUNKS, depth),
+            b16(place, 2, count, m * place * rows),
+            f32(place, 2, count, pair),
+            b16(place, count, pair),
             b16(place, count, pair),
             b16(place, count, pair),
             b16(place, count, pair),
@@ -658,13 +753,15 @@
         + dma(2 * spans, place)
         + dma(levels - 1, CHUNKS)
         + dma(levels, CHUNKS)
-        + dma(n - 1)
+        + dma(n)
         + dma(place)
         + dma(heads, place)
         + dma(levels, CHUNKS)
         + dma(levels - 1, CHUNKS)
-        + dma(place)
-        + dma(spans - 1, place)
+        + dma(levels - 1)
+        + dma(m - 1, place)
+        + dma(spans - 1, place + 1)
+        + dma(spans, place + 1)
         + dma(place)
         + dma(place - 1)
         + dma(m - 1)

time: 92.6 us -> 85.4 us (0.922)
  Pallas kernels: 91.6 us -> 84.5 us
    pallas_call x1, Pallas kernels: 89.8 us -> 82.6 us  [run(): pl.pallas_call(functools.partial(whole_kernel, n, m), out_shape=[jax.Shap...]
where the time goes in v3:
time: 85.4 us; the launch traced here: 85.3 us
  Pallas kernels  84.5 us (99%)
    pallas_call x1, Pallas kernels, run(): pl.pallas_call(functools.partial(whole_kernel, n, m), out_shape=[jax.Shap...  82.6 us
    pallas_call x1, Pallas kernels, finish(): pl.pallas_call(finish_kernel, out_shape=[jax.ShapeDtypeStruct(a.shape, a....  1.86 us

profile of v3, /device:TPU:0, one launch (start us, length us, event | category | flops | bytes accessed | tf_op | source)
XLA Modules:
  0.0 85.3 jit_solution(3798841879619728937)
XLA Ops:
  0.6 82.6 %whole.1 = (bf16[1024,2,128]{2,1,0:T(2,128)(2,1)S(1)}, bf16[1024,2,128]{2,1,0:T(2,128)(2,1)S(1)}, bf16[128,2048]{1,0:T(8,128)(2,1)S(1)}, f32[64,2048]{1,0:T(8,128)S(1)}, f32[2,8,128]{2,1,0:T(8,128)S(1)}) custom-call(f32[2]{0:T(128)} %lam_in.1, bf16[128,2048]{1,0:T(8,128)(2,1)} %bitcast.7, bf16[128,2048]{1,0:T(8,128)(2,1)} %bitcast.8, ...), custom_call_target="tpu_custom_call" | custom-call | tf_op jit(solution)/shard_map/whole/pallas_call | solution.py:774
  83.3 1.9 %finish.1 = (bf16[1024,2,128]{2,1,0:T(2,128)(2,1)}, bf16[1024,2,128]{2,1,0:T(2,128)(2,1)}, bf16[128,2048]{1,0:T(8,128)(2,1)}, f32[64,2048]{1,0:T(8,128)}, f32[2]{0:T(128)}) custom-call(bf16[1024,2,128]{2,1,0:T(2,128)(2,1)S(1)} %get-tuple-element.15.gq_ref, bf16[1024,2,128]{2,1,0:T(2,128)(2,1)S(1)} %get-tuple-element.16.gk_ref, ...), custom_call_target="tpu_custom_call" | custom-call | tf_op jit(solution)/shard_map/finish/pallas_call | solution.py:678

commit v4 on v3

--- a/solution.py
+++ b/solution.py
@@ -51,7 +51,7 @@
         self.lam_ref, self.q_ref, self.k_ref = lam_ref, q_ref, k_ref
         self.v_ref, self.g_ref, self.width = v_ref, g_ref, width
         self.p_ref, self.a_ref, self.qh_ref, self.kt_ref, self.go_ref = bufs[:5]
-        self.gv_acc, self.gk_acc = bufs[5:]
+        self.gv_acc, self.gk_acc, self.vt_ref, self.gt_ref = bufs[5:]
         self.gq_ref, self.gk_ref, self.gl_ref = outs
         self.length = q_ref.shape[0]
         self.block = min(QBLOCK, self.length)
@@ -104,16 +104,22 @@
         for (lo, hi), p1, p2 in zip(pieces, *probs):
             self.a_ref[head, base + lo : base + hi] = (p1 - lam * p2).astype(BF16)
 
+    def turn_cotangent(self, head):
+        wide = self.g_ref[:, :, self.columns(head)].reshape(self.length, self.width)
+        self.gt_ref[head] = wide.astype(F32).T
+
+    def turn_values(self, head, half):
+        size = self.length // 2
+        span = pl.ds(pl.multiple_of(half * size, size), size)
+        values = self.v_ref[half, :, :, self.columns(head)].reshape(size, self.width)
+        self.vt_ref[head, :, span] = values.astype(F32).T.astype(BF16)
+
     def values_grad(self, head):
-        width = self.width
-        v_all = self.v_ref[:, :, :, self.columns(head)].reshape(self.length, width)
-        vt = v_all.astype(F32).T.astype(BF16)
-        gt = self.g_ref[:, :, self.columns(head)].reshape(self.length, width).astype(F32).T
         for index in range(self.count):
             off, reach, pieces, base = self.span(index)
             weights = self.a_ref[head, base : base + reach]
-            out_t = dot_nn(vt[:, :reach], weights)
-            cot = gt[:, off:reach]
+            out_t = dot_nn(self.vt_ref[head, :, :reach], weights)
+            cot = self.gt_ref[head, :, off:reach]
             inverse = lax.rsqrt(jnp.mean(out_t * out_t, axis=0, keepdims=True) + EPS)
             normed = out_t * inverse
             grad_out = (
@@ -171,12 +177,12 @@
     n, m,
     lam_in, tok_ref, cot_ref, w_ref, q_ref, k_ref,
     gq_ref, gk_ref, gt_ref, gw_ref, glo_ref,
-    lam_ref, q_nat, k_nat, qf, kf, gqf, gkf,
-    tokens, tok_t, wc, coth, vloc, v_ref, p_ref, a_ref, qh_ref, kt_ref, go_ref, gv_acc, gk_acc,
+    lam_ref, qf, kf,
+    vt_ref, gt_f, wct, tokens, tok_t, wc, coth, vloc, v_ref, p_ref, a_ref, qh_ref, kt_ref, go_ref, sum_acc,
     gvb, dv, part, ry, sz, rz, rzd, tokx, acc, sb, rc, sc, rd, gl_ref, lbuf,
-    local_sem, wa_s, wa_r, wx_s, wx_r, wd_s, wd_r, tz_s, tz_r, ty_s, ty_r,
-    c_s, c_r, v_s, v_r, dv_s, dv_r, y_s, y_r, z_s, z_r, zd_s, zd_r, tx_s, tx_r, gx_s, gx_r, gd_s, gd_r, e_s, e_r,
-    d_s, d_r, l_s, l_r,
+    local_sem, send_sem, wa_r, wx_r, wd_r, tz_r, ty_r,
+    c_r, v_r, dv_r, y_r, z_r, zd_r, tx_r, gx_r, gd_r, e_r,
+    d_r, l_r,
 ):
     me = lax.axis_index("sp")
     dp = lax.axis_index("dp")
@@ -202,7 +208,26 @@
     in_half = [(pos + k) % place for k in range(1, place)]
     sp_peers = [(me + k) % n for k in range(1, n)]
     dp_peers = [(dp + k) % m for k in range(1, m)]
-    done = []
+    sent = []
+    unit = p_ref.shape[3] * 4
+    limit = p_ref.shape[2] * unit
+
+    def size_of(ref):
+        return math.prod(ref.shape) * jnp.dtype(ref.dtype).itemsize
+
+    def wait_bytes(sem, size):
+        if size <= limit:
+            ref = p_ref.at[0, 0, pl.ds(0, size // unit)]
+        else:
+            ref = p_ref.at[0, :, pl.ds(0, size // unit // 2)]
+        pltpu.make_async_copy(ref, ref, sem).wait()
+
+    def send(src, dst, recv, sp, dp):
+        size = size_of(src)
+        if not sent or sent[-1] + size > limit:
+            sent.append(0)
+        sent[-1] += size
+        return remote(src, dst, send_sem.at[len(sent) - 1], recv, sp, dp)
 
     def lane(start, size):
         return pl.ds(pl.multiple_of(start, size), size)
@@ -218,25 +243,23 @@
         )
         for j in range(2)
     ] + [
-        pltpu.make_async_copy(q_ref, q_nat, local_sem.at[4]),
-        pltpu.make_async_copy(k_ref, k_nat, local_sem.at[5]),
+        pltpu.make_async_copy(q_ref, gq_ref, local_sem.at[4]),
+        pltpu.make_async_copy(k_ref, gk_ref, local_sem.at[5]),
         pltpu.make_async_copy(lam_in, lam_ref, local_sem.at[6]),
     ]
     greet([(s, dp) for s in sp_peers] + [(me, d) for d in dp_peers], locals_)
 
     def begin(copy):
         copy.start()
-        done.append(copy)
         return copy
 
     def weight_out(k, s, j):
         start = (j * place + s % place) * feats
         return begin(
-            remote(
+            send(
                 w_ref.at[:, lane(start, feats)],
                 wc.at[me, dp, :, pl.ds(j * feats, feats)],
-                wa_s.at[k, j],
-                wa_r.at[k, j],
+                wa_r.at[min(k, place)],
                 s,
                 dp,
             )
@@ -247,10 +270,9 @@
 
     def tok_up(k, c):
         return begin(
-            remote(
+            send(
                 tok_ref.at[chunk(c)],
                 tokens.at[pos, chunk(c)],
-                tz_s.at[k, c],
                 tz_r.at[k, c],
                 at_pos(ups[k] * 2 + y),
                 dp,
@@ -260,23 +282,19 @@
     def tok_side(slot, origin, c):
         src = tok_ref.at[chunk(c)] if slot == 0 else tokens.at[origin, chunk(c)]
         return begin(
-            remote(
+            send(
                 src,
                 tokens.at[origin, chunk(c)],
-                ty_s.at[slot, c],
-                ty_r.at[slot, c],
+                ty_r.at[slot],
                 beside,
                 dp,
             )
         )
 
     def cot_out(k, s):
-        return remote(
-            cot_ref.at[:, lane(s * feats, feats)], coth.at[me], c_s.at[k], c_r.at[me], s, dp
-        )
-
-    def cot_in(s):
-        return remote(coth.at[s], coth.at[s], c_s.at[0], c_r.at[s], s, dp)
+        return send(
+            cot_ref.at[:, lane(s * feats, feats)], coth.at[me], c_r.at[0], s, dp
+        )
 
     far = [(1 - half) * place + (pos + k) % place for k in range(place)]
     near = [at_pos(p) for p in in_half]
@@ -298,18 +316,17 @@
         for i in range(2)
     ]
     near_cots = [cot_out(place + k, s) for k, s in enumerate(near)]
-    done.extend(far_cots + near_cots)
     for copy in far_cots:
         copy.start()
     att = Attention(
         lam_ref, qf, kf, v_ref, coth,
-        (p_ref, a_ref, qh_ref, kt_ref, go_ref, gv_acc, gk_acc),
-        (gqf, gkf, gl_ref), width,
+        (p_ref, a_ref, qh_ref, kt_ref, go_ref, sum_acc, sum_acc, vt_ref, gt_f),
+        (qf, kf, gl_ref), width,
     )
     for copy in locals_[4:]:
         copy.wait()
-    qf[...] = q_nat[...].reshape(length, feats)
-    kf[...] = k_nat[...].reshape(length, feats)
+    qf[...] = gq_ref[...].reshape(length, feats)
+    kf[...] = gk_ref[...].reshape(length, feats)
     pieces = [(h, i) for h in range(heads) for i in range(att.count)]
     for h in range(heads):
         att.prepare(h)
@@ -322,20 +339,20 @@
 
     for copy in locals_[2:4]:
         copy.wait()
-    for copy in wa:
-        copy.wait_recv()
+    piece = size_of(w_ref) // n
+    wait_bytes(wa_r.at[place], piece * len(wa))
     wx, wd = {}, []
 
     def core_out(slot, p, block):
         wd.append(
-            begin(remote(block, block, wd_s.at[slot, p], wd_r.at[slot, p], me, other))
+            begin(send(block, block, wd_r.at[0], me, other))
         )
 
     def x_out(j, p, block):
         for k, xk in enumerate(xs):
             wx[j, k, p] = begin(
-                remote(
-                    block, block, wx_s.at[j, k, p], wx_r.at[j, k, p], me, xk * 2 + core
+                send(
+                    block, block, wx_r.at[j, k, p], me, xk * 2 + core
                 )
             )
 
@@ -364,11 +381,10 @@
         stretch = lane((dp * place + b) * rows, rows)
         for k, d in enumerate(dp_peers):
             txs[k, slot] = begin(
-                remote(
+                send(
                     tok_t.at[b, :, :, d],
                     tokx.at[:, :, :, stretch],
-                    tx_s.at[k, slot],
-                    tx_r.at[k, slot],
+                    tx_r.at[0],
                     me,
                     d,
                 )
@@ -383,8 +399,7 @@
             core_out(slot, p, wc_block(h, q, origin * 2 + core))
 
     for k in range(place):
-        for copy in wb[k]:
-            copy.wait_recv()
+        wait_bytes(wa_r.at[k], piece * len(wb[k]))
         block = wc_block(1 - half, (pos + place - k) % place, dp)
         x_out(1, k, block)
         core_out(spans, k, block)
@@ -402,46 +417,54 @@
         copy.start()
     for k in range(levels - 1):
         turn(1 + k, downs[k] * 2 + y)
-    for copy in own:
-        copy.wait_recv()
+    wait_bytes(ty_r.at[0], size_of(tok_ref))
     turn(levels, level * 2 + 1 - y)
-    for copy in wd:
-        copy.wait_recv()
+    wait_bytes(wd_r.at[0], 2 * piece * len(wd))
 
     def weight():
         return wc[...].reshape(depth, 2 * feats)
 
     def values_of(b, k):
         vloc[b] = dot_nn(tokens[b], weight()).astype(BF16)
-        copy = begin(
-            remote(
-                vloc.at[b, :, lane((1 - half) * feats, feats)],
-                v_ref.at[half, b],
-                v_s.at[k],
-                v_r.at[k],
-                partner,
-                dp,
-            )
-        )
         v_ref[half, b] = vloc[b, :, lane(half * feats, feats)]
-        return copy
-
-    v_copies = [values_of(pos, 0)]
+
+    def values_out(blocks):
+        for h in range(heads):
+            for b, k in blocks:
+                v_copies[h, k] = begin(
+                    send(
+                        vloc.at[b, :, lane((1 - half) * feats + h * width, width)],
+                        v_ref.at[half, b, :, pl.ds(h * width, width)],
+                        v_r.at[h],
+                        partner,
+                        dp,
+                    )
+                )
+
+    v_copies = {}
+    blocks = (
+        [(pos, 0)]
+        + [(downs[k] * 2 + y, 1 + k) for k in range(levels - 1)]
+        + [(level * 2 + 1 - y, levels)]
+    )
+    for b, k in blocks:
+        values_of(b, k)
+    values_out(blocks)
+    wct[...] = weight().astype(F32).T.astype(BF16)
     for k in range(levels - 1):
-        v_copies.append(values_of(downs[k] * 2 + y, 1 + k))
-    v_copies.append(values_of(level * 2 + 1 - y, levels))
-    for k in range(levels - 1):
-        for c in range(CHUNKS):
-            side[k, c].wait_recv()
-        v_copies.append(values_of(downs[k] * 2 + 1 - y, levels + 1 + k))
+        wait_bytes(ty_r.at[1 + k], size_of(tok_ref))
+        b = downs[k] * 2 + 1 - y
+        values_of(b, levels + 1 + k)
+        values_out([(b, levels + 1 + k)])
 
     for k in range(levels - 1):
         turn(levels + 1 + k, downs[k] * 2 + 1 - y)
-    for copy in v_copies:
-        copy.wait_recv()
     locals_[1].wait()
-    for s in sp_peers:
-        cot_in(s).wait_recv()
+    wait_bytes(c_r.at[0], size_of(cot_ref) // n * (n - 1))
+    for h in range(heads):
+        att.turn_cotangent(h)
+    for h in range(heads):
+        att.turn_values(h, half)
 
     order = (
         [u * 2 + 1 - y for u in ups] + [level * 2 + 1 - y] + [u * 2 + y for u in ups] + [pos]
@@ -450,24 +473,26 @@
 
     def dv_out(h, k):
         dv_copies[h, k] = begin(
-            remote(
+            send(
                 gvb.at[h, 1 - half, order[k]],
                 dv.at[dp, order[k], :, lane(half * feats + h * width, width)],
-                dv_s.at[h, k],
-                dv_r.at[h, k],
+                dv_r.at[k],
                 partner,
                 dp,
             )
         )
 
     for h in range(heads):
+        wait_bytes(v_r.at[h], size_of(v_ref) // 2 // heads)
+        att.turn_values(h, 1 - half)
         att.values_grad(h)
-        gvb[h] = gv_acc[...].astype(BF16).reshape(2, place, rows, width)
+        gvb[h] = sum_acc[...].astype(BF16).reshape(2, place, rows, width)
         dv_out(h, 0)
+    for h in range(heads):
         for b in range(place):
             dv[dp, b, :, lane(half * feats + h * width, width)] = gvb[h, half, b]
 
-    gxs, gds = {}, []
+    gxs, gds = {}, {}
 
     def share(d, j):
         if j == 0:
@@ -475,21 +500,16 @@
         return dv.at[d, order[j - 1], :, lane((1 - half) * feats, feats)]
 
     def share_core(slot, j, d):
-        gds.append(
-            begin(
-                remote(
-                    share(d, j), share(d, j), gd_s.at[slot, j], gd_r.at[slot, j], me, other
-                )
-            )
+        gds[slot, j] = begin(
+            send(share(d, j), share(d, j), gd_r.at[min(j, 1)], me, other)
         )
 
     def share_out(j):
         for k, xk in enumerate(xs):
             gxs[k, j] = begin(
-                remote(
+                send(
                     share(dp, j),
                     share(dp, j),
-                    gx_s.at[k, j],
                     gx_r.at[k, j],
                     me,
                     xk * 2 + core,
@@ -514,23 +534,21 @@
         att.scores_grad(h, dv_more if h == 0 else None)
 
     def dv_wait(k):
-        for h in range(heads):
-            dv_copies[h, k].wait_recv()
+        wait_bytes(dv_r.at[k], rows * feats * 2)
         share_out(1 + k)
 
     def partial(k):
-        part[order[k]] = dot_nt(dv[dp, order[k]], weight()).astype(BF16)
+        part[order[k]] = dot_nn(dv[dp, order[k]], wct[...]).astype(BF16)
 
     ys, zs, zd = {}, {}, {}
     last = CHUNKS - 1
 
     def y_out(k, c):
         ys[k, c] = begin(
-            remote(
+            send(
                 part.at[order[k], chunk(c)],
                 ry.at[k, chunk(c)],
-                y_s.at[k, c],
-                y_r.at[k, c],
+                y_r.at[min(k * CHUNKS + c, (levels - 1) * CHUNKS)],
                 beside,
                 dp,
             )
@@ -547,10 +565,9 @@
             y_out(k, c)
         if k < levels - 1:
             zd[k] = begin(
-                remote(
+                send(
                     part.at[order[k], chunk(last)],
                     rzd.at[k],
-                    zd_s.at[k],
                     zd_r.at[k],
                     at_pos(ups[k] * 2 + y),
                     dp,
@@ -559,7 +576,7 @@
     for h in range(split, heads):
         att.scores_grad(h)
     ls = [
-        begin(remote(gl_ref, lbuf.at[k], l_s.at[k], l_r.at[k], me, d))
+        begin(remote(gl_ref, lbuf.at[k], send_sem.at[7], l_r.at[0], me, d))
         for k, d in enumerate(dp_peers)
     ]
     def last_out():
@@ -578,16 +595,16 @@
                 total = total + ry[k, chunk(c)].astype(F32)
             sz[k, chunk(c)] = total.astype(BF16)
             zs[k, c] = begin(
-                remote(
+                send(
                     sz.at[k, chunk(c)],
                     rz.at[k, chunk(c)],
-                    z_s.at[k, c],
-                    z_r.at[k, c],
+                    z_r.at[k],
                     at_pos(ups[k] * 2 + y),
                     dp,
                 )
             )
 
+    share_on(0)
     for k in range(levels, 2 * levels - 1):
         dv_wait(k)
         partial(k)
@@ -595,66 +612,73 @@
     rows_up(0)
     last_out()
     dv_wait(2 * levels - 1)
-    for j in range(place):
+    wait_bytes(tx_r.at[0], size_of(tokx) // m * (m - 1))
+    wait_bytes(gd_r.at[0], size_of(dv) // 2 // m * spans)
+
+    es, ds_ = {}, {}
+    turns = in_half + [pos]
+
+    def term(j, side_half):
+        cols = lane(side_half * feats, feats)
+        total = dot_nn(
+            tokx[...].reshape(place * 2 * count, m * place * rows),
+            dv[:, :, :, cols].reshape(m * place * rows, feats),
+        )
+        acc[:, :, :, cols] = total.reshape(place, 2, count, feats)
+        for k, p in enumerate(turns):
+            sb[p, :, cols] = acc[p, 1 - half, :, cols].astype(BF16)
+            es[j, k] = begin(
+                send(
+                    sb.at[p, :, cols], rc.at[p, :, cols], e_r.at[k], partner, dp
+                )
+            )
+
+    term(0, half)
+    for j in range(1, place):
         share_on(j)
     for c in range(1, last - 1):
         rows_up(c)
     share_on(place)
-    for k in range(m - 1):
-        for slot in range(place):
-            txs[k, slot].wait_recv()
-    for copy in gds:
-        copy.wait_recv()
-
-    es, ds_ = {}, {}
-    turns = in_half + [pos]
-    dv_all = dv[...].reshape(m * place * rows, 2 * feats)
-    for k, p in enumerate(turns):
-        acc[p] = dot_nn(tokx[p].reshape(2 * count, m * place * rows), dv_all).reshape(
-            2, count, 2 * feats
-        )
-        sb[p] = acc[p, 1 - half].astype(BF16)
-        es[k] = begin(remote(sb.at[p], rc.at[p], e_s.at[k], e_r.at[k], partner, dp))
+    wait_bytes(gd_r.at[1], size_of(dv) // 2 // m * spans)
+    term(1, 1 - half)
     rows_up(last - 1)
     partial(2 * levels - 1)
 
     def finish(k):
         p = turns[k]
-        es[k].wait_recv()
+        wait_bytes(e_r.at[k], size_of(rc) // place)
         total = (acc[p, half] + rc[p].astype(F32)).astype(BF16)
         if k < place - 1:
             sc[p] = total
             ds_[k] = begin(
-                remote(sc.at[p], rd.at[pos], d_s.at[k], d_r.at[k], at_pos(p), dp)
+                send(sc.at[p], rd.at[pos], d_r.at[0], at_pos(p), dp)
             )
         else:
             rd[pos] = total
 
-    gq_ref[...] = gqf[...].reshape(gq_ref.shape)
-    gk_ref[...] = gkf[...].reshape(gk_ref.shape)
+    gq_ref[...] = qf[...].reshape(gq_ref.shape)
+    gk_ref[...] = kf[...].reshape(gk_ref.shape)
     for k in range(place):
         finish(k)
-    for c in range(CHUNKS):
-        total = part[pos, chunk(c)].astype(F32)
-        ys[levels - 1, c].wait_recv()
-        total = total + ry[levels - 1, chunk(c)].astype(F32)
-        for k in range(levels - 1):
-            zs[k, c].wait_recv()
-            total = total + rz[k, chunk(c)].astype(F32)
-        gt_ref[chunk(c)] = total.astype(BF16)
+    wait_bytes(y_r.at[(levels - 1) * CHUNKS], size_of(tok_ref))
+    total = part[pos].astype(F32) + ry[levels - 1].astype(F32)
+    for k in range(levels - 1):
+        wait_bytes(z_r.at[k], size_of(tok_ref))
+        total = total + rz[k].astype(F32)
+    gt_ref[...] = total.astype(BF16)
     lam = gl_ref[...]
+    pltpu.make_async_copy(lbuf, lbuf, l_r.at[0]).wait()
     for k in range(m - 1):
-        ls[k].wait_recv()
         lam = lam + lbuf[k]
     glo_ref[...] = lam
-    for k in range(place - 1):
-        ds_[k].wait_recv()
+    wait_bytes(d_r.at[0], size_of(rd) // place * (place - 1))
     for p in range(place):
         for j in range(2):
             start = (j * place + p) * feats
             gw_ref[:, start : start + feats] = rd[p, :, j * feats : (j + 1) * feats].astype(F32)
-    for copy in done:
-        copy.wait_send()
+    pltpu.make_async_copy(lbuf, lbuf, send_sem.at[7]).wait()
+    for g, size in enumerate(sent):
+        wait_bytes(send_sem.at[g], size)
 
 
 def finish_kernel(gq_ref, gk_ref, gt_ref, gw_ref, gl_ref, *refs):
@@ -707,17 +731,16 @@
         return pltpu.VMEM(shape, F32)
 
     def dma(*shape):
-        return [pltpu.SemaphoreType.DMA(tuple(max(s, 1) for s in shape))] * 2
+        return [pltpu.SemaphoreType.DMA(tuple(max(s, 1) for s in shape))]
 
     scratch = (
         [
             pltpu.SMEM((heads,), F32),
-            b16(length, heads, width),
-            b16(length, heads, width),
             b16(length, feats),
             b16(length, feats),
-            b16(length, feats),
-            b16(length, feats),
+            b16(heads, width, length),
+            f32(heads, width, length),
+            b16(pair, depth),
             b16(place, rows, depth),
             b16(place, place, 2, m, count, rows),
             b16(n, m, count, pair),
@@ -729,7 +752,6 @@
             b16(heads, 2, length, width),
             b16(heads, 2, width, length),
             b16(heads, width, length),
-            f32(length, width),
             f32(length, width),
             b16(heads, 2, place, rows, width),
             b16(m, place, rows, pair),
@@ -748,23 +770,24 @@
             f32(m - 1, heads, 8, 128),
             pltpu.SemaphoreType.DMA((7,)),
         ]
-        + dma(n - 1, 2)
+        + dma(8)
+        + dma(place + 1)
         + dma(2, spans - 1, place)
-        + dma(2 * spans, place)
+        + dma(1)
         + dma(levels - 1, CHUNKS)
-        + dma(levels, CHUNKS)
-        + dma(n)
+        + dma(levels)
+        + dma(1)
+        + dma(heads)
         + dma(place)
-        + dma(heads, place)
-        + dma(levels, CHUNKS)
-        + dma(levels - 1, CHUNKS)
+        + dma((levels - 1) * CHUNKS + 1)
         + dma(levels - 1)
-        + dma(m - 1, place)
+        + dma(levels - 1)
+        + dma(1)
         + dma(spans - 1, place + 1)
-        + dma(spans, place + 1)
+        + dma(2)
         + dma(place)
-        + dma(place - 1)
-        + dma(m - 1)
+        + dma(1)
+        + dma(1)
     )
     held = sum(
         math.prod(ref.shape) * jnp.dtype(ref.dtype).itemsize

time: 85.4 us -> 81.9 us (0.959)
  Pallas kernels: 84.5 us -> 81 us
    pallas_call x1, Pallas kernels: 82.6 us -> 79.1 us  [run(): pl.pallas_call(functools.partial(whole_kernel, n, m), out_shape=[jax.Shap...]
where the time goes in v4:
time: 81.9 us; the launch traced here: 81.8 us
  Pallas kernels  81 us (99%)
    pallas_call x1, Pallas kernels, run(): pl.pallas_call(functools.partial(whole_kernel, n, m), out_shape=[jax.Shap...  79.1 us
    pallas_call x1, Pallas kernels, finish(): pl.pallas_call(finish_kernel, out_shape=[jax.ShapeDtypeStruct(a.shape, a....  1.86 us

profile of v4, /device:TPU:0, one launch (start us, length us, event | category | flops | bytes accessed | tf_op | source)
XLA Modules:
  0.0 81.8 jit_solution(8444797198367110289)
XLA Ops:
  0.6 79.1 %whole.1 = (bf16[1024,2,128]{2,1,0:T(2,128)(2,1)S(1)}, bf16[1024,2,128]{2,1,0:T(2,128)(2,1)S(1)}, bf16[128,2048]{1,0:T(8,128)(2,1)S(1)}, f32[64,2048]{1,0:T(8,128)S(1)}, f32[2,8,128]{2,1,0:T(8,128)S(1)}) custom-call(f32[2]{0:T(128)} %lam_in.1, bf16[128,2048]{1,0:T(8,128)(2,1)} %bitcast.7, bf16[128,2048]{1,0:T(8,128)(2,1)} %bitcast.8, ...), custom_call_target="tpu_custom_call" | custom-call | tf_op jit(solution)/shard_map/whole/pallas_call | solution.py:797
  79.8 1.9 %finish.1 = (bf16[1024,2,128]{2,1,0:T(2,128)(2,1)}, bf16[1024,2,128]{2,1,0:T(2,128)(2,1)}, bf16[128,2048]{1,0:T(8,128)(2,1)}, f32[64,2048]{1,0:T(8,128)}, f32[2]{0:T(128)}) custom-call(bf16[1024,2,128]{2,1,0:T(2,128)(2,1)S(1)} %get-tuple-element.15.gq_ref, bf16[1024,2,128]{2,1,0:T(2,128)(2,1)S(1)} %get-tuple-element.16.gk_ref, ...), custom_call_target="tpu_custom_call" | custom-call | tf_op jit(solution)/shard_map/finish/pallas_call | solution.py:702

commit v5 on v4

--- a/solution.py
+++ b/solution.py
@@ -179,9 +179,9 @@
     gq_ref, gk_ref, gt_ref, gw_ref, glo_ref,
     lam_ref, qf, kf,
     vt_ref, gt_f, wct, tokens, tok_t, wc, coth, vloc, v_ref, p_ref, a_ref, qh_ref, kt_ref, go_ref, sum_acc,
-    gvb, dv, part, ry, sz, rz, rzd, tokx, acc, sb, rc, sc, rd, gl_ref, lbuf,
+    gvb, dv, part, ry, sz, rz, tokx, acc, sb, rc, sc, rd, gl_ref, lbuf,
     local_sem, send_sem, wa_r, wx_r, wd_r, tz_r, ty_r,
-    c_r, v_r, dv_r, y_r, z_r, zd_r, tx_r, gx_r, gd_r, e_r,
+    c_r, v_r, dv_r, y_r, z_r, tx_r, gx_r, gd_r, e_r,
     d_r, l_r,
 ):
     me = lax.axis_index("sp")
@@ -540,8 +540,7 @@
     def partial(k):
         part[order[k]] = dot_nn(dv[dp, order[k]], wct[...]).astype(BF16)
 
-    ys, zs, zd = {}, {}, {}
-    last = CHUNKS - 1
+    ys, zs = {}, {}
 
     def y_out(k, c):
         ys[k, c] = begin(
@@ -561,38 +560,19 @@
                 for j in range(levels, 2 * levels):
                     dv_out(h, j)
         partial(k)
-        for c in range(last):
+        for c in range(CHUNKS):
             y_out(k, c)
-        if k < levels - 1:
-            zd[k] = begin(
-                send(
-                    part.at[order[k], chunk(last)],
-                    rzd.at[k],
-                    zd_r.at[k],
-                    at_pos(ups[k] * 2 + y),
-                    dp,
-                )
-            )
     for h in range(split, heads):
         att.scores_grad(h)
     ls = [
         begin(remote(gl_ref, lbuf.at[k], send_sem.at[7], l_r.at[0], me, d))
         for k, d in enumerate(dp_peers)
     ]
-    def last_out():
-        total = part[order[levels - 1], chunk(last)].astype(F32)
-        for k in range(levels - 1):
-            zd[k].wait_recv()
-            total = total + rzd[k].astype(F32)
-        part[order[levels - 1], chunk(last)] = total.astype(BF16)
-        y_out(levels - 1, last)
-
     def rows_up(c):
         for k in range(levels - 1):
             total = part[ups[k] * 2 + y, chunk(c)].astype(F32)
-            if c < last:
-                ys[k, c].wait_recv()
-                total = total + ry[k, chunk(c)].astype(F32)
+            ys[k, c].wait_recv()
+            total = total + ry[k, chunk(c)].astype(F32)
             sz[k, chunk(c)] = total.astype(BF16)
             zs[k, c] = begin(
                 send(
@@ -608,9 +588,7 @@
     for k in range(levels, 2 * levels - 1):
         dv_wait(k)
         partial(k)
-    rows_up(last)
     rows_up(0)
-    last_out()
     dv_wait(2 * levels - 1)
     wait_bytes(tx_r.at[0], size_of(tokx) // m * (m - 1))
     wait_bytes(gd_r.at[0], size_of(dv) // 2 // m * spans)
@@ -636,12 +614,12 @@
     term(0, half)
     for j in range(1, place):
         share_on(j)
-    for c in range(1, last - 1):
+    for c in range(1, CHUNKS - 1):
         rows_up(c)
     share_on(place)
     wait_bytes(gd_r.at[1], size_of(dv) // 2 // m * spans)
     term(1, 1 - half)
-    rows_up(last - 1)
+    rows_up(CHUNKS - 1)
     partial(2 * levels - 1)
 
     def finish(k):
@@ -684,8 +662,10 @@
 def finish_kernel(gq_ref, gk_ref, gt_ref, gw_ref, gl_ref, *refs):
     outs, lam_out, sems = refs[:4], refs[4], refs[5]
     copies = [
-        pltpu.make_async_copy(src, dst, sems.at[i])
+        pltpu.make_async_copy(src.at[part], dst.at[part], sems.at[2 * i + j])
         for i, (src, dst) in enumerate(zip((gq_ref, gk_ref, gt_ref, gw_ref), outs))
+        for j in range(2)
+        for part in [pl.ds(j * (src.shape[0] // 2), src.shape[0] // 2)]
     ]
     for copy in copies:
         copy.start()
@@ -705,7 +685,7 @@
         + [jax.ShapeDtypeStruct(gl.shape[:1], F32)],
         in_specs=[vmem] * 5,
         out_specs=[hbm] * 4 + [pl.BlockSpec(memory_space=pltpu.SMEM)],
-        scratch_shapes=[pltpu.SemaphoreType.DMA((4,))],
+        scratch_shapes=[pltpu.SemaphoreType.DMA((8,))],
         compiler_params=pltpu.CompilerParams(vmem_limit_bytes=2 * 1024 * 1024),
         name="finish",
     )(*results, gl)
@@ -759,7 +739,6 @@
             b16(levels, rows, depth),
             b16(max(levels - 1, 1), rows, depth),
             b16(max(levels - 1, 1), rows, depth),
-            b16(max(levels - 1, 1), rows // CHUNKS, depth),
             b16(place, 2, count, m * place * rows),
             f32(place, 2, count, pair),
             b16(place, count, pair),
@@ -780,7 +759,6 @@
         + dma(heads)
         + dma(place)
         + dma((levels - 1) * CHUNKS + 1)
-        + dma(levels - 1)
         + dma(levels - 1)
         + dma(1)
         + dma(spans - 1, place + 1)

time: 81.9 us -> 82.3 us (level)
  no operation moved by 1% of the time
where the time goes in v5:
time: 82.3 us; the launch traced here: 82.1 us
  Pallas kernels  81.3 us (99%)
    pallas_call x1, Pallas kernels, run(): pl.pallas_call(functools.partial(whole_kernel, n, m), out_shape=[jax.Shap...  79.5 us
    pallas_call x1, Pallas kernels, finish(): pl.pallas_call(finish_kernel, out_shape=[jax.ShapeDtypeStruct(a.shape, a....  1.9 us

profile of v5, /device:TPU:0, one launch (start us, length us, event | category | flops | bytes accessed | tf_op | source)
XLA Modules:
  0.0 82.1 jit_solution(10468401415773475811)
XLA Ops:
  0.6 79.5 %whole.1 = (bf16[1024,2,128]{2,1,0:T(2,128)(2,1)S(1)}, bf16[1024,2,128]{2,1,0:T(2,128)(2,1)S(1)}, bf16[128,2048]{1,0:T(8,128)(2,1)S(1)}, f32[64,2048]{1,0:T(8,128)S(1)}, f32[2,8,128]{2,1,0:T(8,128)S(1)}) custom-call(f32[2]{0:T(128)} %lam_in.1, bf16[128,2048]{1,0:T(8,128)(2,1)} %bitcast.7, bf16[128,2048]{1,0:T(8,128)(2,1)} %bitcast.8, ...), custom_call_target="tpu_custom_call" | custom-call | tf_op jit(solution)/shard_map/whole/pallas_call | solution.py:775
  80.1 1.9 %finish.1 = (bf16[1024,2,128]{2,1,0:T(2,128)(2,1)}, bf16[1024,2,128]{2,1,0:T(2,128)(2,1)}, bf16[128,2048]{1,0:T(8,128)(2,1)}, f32[64,2048]{1,0:T(8,128)}, f32[2]{0:T(128)}) custom-call(bf16[1024,2,128]{2,1,0:T(2,128)(2,1)S(1)} %get-tuple-element.15.gq_ref, bf16[1024,2,128]{2,1,0:T(2,128)(2,1)S(1)} %get-tuple-element.16.gk_ref, ...), custom_call_target="tpu_custom_call" | custom-call | tf_op jit(solution)/shard_map/finish/pallas_call | solution.py:682
